TPU v7x, 32 devices: a whole 2x2x4 slice. The times are simulated.
32 devices in a mesh: rep: 2 (over x), fs: 8 (over z, y), tp: 2 (over core).
Axes of the slice: x: 2, y: 2, z: 4, core: 2. Of those that a mesh axis runs over, the one named last changes fastest.
Arguments:
- block_input: bfloat16 [8192, 2048], P(('rep', 'fs', 'tp')), may hold values from -6 to 6
- pre_gain: float32 [2048], replicated, may hold values from 0.1 to 1.9
- post_gain: float32 [2048], replicated, may hold values from 0.1 to 1.9
- gate_saved: bfloat16 [8192, 5632], P(('rep', 'fs'), 'tp'), may hold values from -8 to 8
- up_saved: bfloat16 [8192, 5632], P(('rep', 'fs'), 'tp'), may hold values from -6 to 6
- branch_saved: bfloat16 [8192, 2048], P(('rep', 'fs', 'tp')), may hold values from -6 to 6
- out_cotangent: bfloat16 [8192, 2048], P(('rep', 'fs', 'tp')), may hold values from -6 to 6
- gate_weight: bfloat16 [2048, 5632], P('fs', 'tp'), may hold values from -0.125 to 0.125
- up_weight: bfloat16 [2048, 5632], P('fs', 'tp'), may hold values from -0.125 to 0.125
- down_weight: bfloat16 [2048, 5632], P('fs', 'tp'), may hold values from -0.078125 to 0.078125
Outputs:
- input_grad: bfloat16 [8192, 2048], P(('rep', 'fs', 'tp'))
- gate_grad: float32 [2048, 5632], P('fs', 'tp')
- up_grad: float32 [2048, 5632], P('fs', 'tp')
- down_grad: float32 [2048, 5632], P('fs', 'tp')
All inputs are finite; a program needn't handle non-finite values.
Results may differ from a plain program's by a relative error of at most 0.018.
Values may be sent and summed in bfloat16 or wider, within the bound.
A program may use at most 128 MiB of HBM per device.

v0:
```python
import functools

import jax
import jax.numpy as jnp
from jax import lax
from jax.sharding import PartitionSpec as P

eps = 1e-06


def contract_rows(left, right):
    return lax.dot_general(
        left, right, (((0,), (0,)), ((), ())), preferred_element_type=jnp.float32
    )


def contract_cols(left, right):
    return lax.dot_general(
        left, right, (((1,), (1,)), ((), ())), preferred_element_type=jnp.float32
    )


def shifted(value, reps, step):
    return lax.ppermute(value, "rep", [(i, (i + step) % reps) for i in range(reps)])


def per_device(
    reps,
    block_input,
    pre_gain,
    post_gain,
    gate_saved,
    up_saved,
    branch_saved,
    out_cotangent,
    gate_weight,
    up_weight,
    down_weight,
):
    bf16, f32 = jnp.bfloat16, jnp.float32
    me = lax.axis_index("rep")
    width = gate_saved.shape[1] // reps

    def columns(value, owner):
        return lax.dynamic_slice_in_dim(value, owner * width, width, axis=1)

    down_full = lax.all_gather(columns(down_weight, me), "fs", axis=0, tiled=True)

    gates = [columns(gate_saved, me)]
    ups = [columns(up_saved, me)]
    for k in range(1, reps):
        there = lax.rem(me + k, reps)
        gates.append(shifted(columns(gate_saved, there), reps, k))
        ups.append(shifted(columns(up_saved, there), reps, k))

    xfull = block_input.astype(f32)
    inv_x = lax.rsqrt(jnp.mean(xfull * xfull, axis=-1, keepdims=True) + eps)
    normed = (xfull * inv_x * pre_gain).astype(bf16)
    branch = branch_saved.astype(f32)
    inv_b = lax.rsqrt(jnp.mean(branch * branch, axis=-1, keepdims=True) + eps)
    upstream = 0.5 * out_cotangent.astype(f32) * post_gain
    branch_grad = (
        inv_b * upstream - branch * inv_b**3 * jnp.mean(upstream * branch, axis=-1, keepdims=True)
    ).astype(bf16)

    normed_own = [normed] + [shifted(normed, reps, k) for k in range(1, reps)]
    branch_own = [branch_grad] + [shifted(branch_grad, reps, k) for k in range(1, reps)]
    normed_rows = [lax.all_gather(v, "tp", axis=0, tiled=True) for v in normed_own]
    branch_rows = [lax.all_gather(v, "tp", axis=0, tiled=True) for v in branch_own]
    normed_all = jnp.concatenate(normed_rows, axis=0)
    branch_all = jnp.concatenate(branch_rows, axis=0)

    gate_f = jnp.concatenate(gates, axis=0).astype(f32)
    up_f = jnp.concatenate(ups, axis=0).astype(f32)
    sigma = jax.nn.sigmoid(gate_f)
    silu_gate = gate_f * sigma
    hidden = (silu_gate * up_f).astype(bf16)

    def spread(total):
        shard = lax.psum_scatter(total.astype(bf16), "fs", scatter_dimension=0, tiled=True)
        out = jnp.zeros((shard.shape[0], width * reps), f32)
        out = lax.dynamic_update_slice_in_dim(out, shard.astype(f32), me * width, axis=1)
        for k in range(1, reps):
            other = shifted(shard, reps, k).astype(f32)
            out = lax.dynamic_update_slice_in_dim(
                out, other, lax.rem(me - k + reps, reps) * width, axis=1
            )
        return out

    down_grad = spread(contract_rows(branch_all, hidden))

    hidden_grad = jnp.dot(branch_all, down_full, preferred_element_type=f32)
    gate_cot = (hidden_grad * up_f * sigma * (1.0 + gate_f * (1.0 - sigma))).astype(bf16)
    up_cot = (hidden_grad * silu_gate).astype(bf16)
    gate_grad = spread(contract_rows(normed_all, gate_cot))
    up_grad = spread(contract_rows(normed_all, up_cot))

    gate_full = lax.all_gather(columns(gate_weight, me), "fs", axis=0, tiled=True)
    up_full = lax.all_gather(columns(up_weight, me), "fs", axis=0, tiled=True)
    partial = (contract_cols(gate_cot, gate_full) + contract_cols(up_cot, up_full)).astype(bf16)
    rows = partial.shape[0] // reps
    normed_grad = None
    for k in range(reps):
        piece = lax.psum_scatter(
            partial[k * rows : (k + 1) * rows], "tp", scatter_dimension=0, tiled=True
        )
        if k:
            piece = shifted(piece, reps, reps - k)
        piece = piece.astype(f32)
        normed_grad = piece if normed_grad is None else normed_grad + piece

    scaled = normed_grad * pre_gain
    input_grad = (
        out_cotangent.astype(f32)
        + inv_x * scaled
        - xfull * inv_x**3 * jnp.mean(scaled * xfull, axis=-1, keepdims=True)
    )
    return (input_grad.astype(bf16), gate_grad, up_grad, down_grad)


def solution(mesh):
    return jax.shard_map(
        functools.partial(per_device, mesh.shape["rep"]),
        mesh=mesh,
        in_specs=(
            P(("rep", "fs", "tp"), None),
            P(),
            P(),
            P(("rep", "fs"), "tp"),
            P(("rep", "fs"), "tp"),
            P(("rep", "fs", "tp"), None),
            P(("rep", "fs", "tp"), None),
            P("fs", "tp"),
            P("fs", "tp"),
            P("fs", "tp"),
        ),
        out_specs=(P(("rep", "fs", "tp"), None), P("fs", "tp"), P("fs", "tp"), P("fs", "tp")),
        check_vma=False,
    )
```

profile of v0, /device:TPU:5, one launch (start us, length us, event | category | flops | bytes accessed | tf_op | source)
XLA Modules:
  0.0 787.9 jit_solution(12480412477546345069)
XLA Ops:
  14.6 23.0 %collective-permute-done = bf16[256,2048]{1,0:T(8,128)(2,1)S(1)} collective-permute-done((bf16[256,2048]{1,0:T(8,128)(2,1)}, bf16[256,2048]{1,0:T(8,128)(2,1)S(1)}, u32[]{:S(2)}, u32[]{:S(2)}) %collective-permute-start) | collective-permute-done | bytes 1048608 | tf_op jit(solution)/shard_map/ppermute | solution.py:24
  49.7 3.5 constant_dynamic-update-slice_fusion.1
  53.2 3.3 constant_dynamic-update-slice_fusion
  56.5 21.4 %collective-permute-done.2 = bf16[512,1408]{1,0:T(8,128)(2,1)} collective-permute-done((bf16[512,1408]{1,0:T(8,128)(2,1)}, bf16[512,1408]{1,0:T(8,128)(2,1)}, u32[]{:S(2)}, u32[]{:S(2)}) %collective-permute-start.2) | collective-permute-done | bytes 1441824 | tf_op jit(solution)/shard_map/ppermute | solution.py:24
  77.9 30.9 %collective-permute-done.1 = bf16[512,1408]{1,0:T(8,128)(2,1)} collective-permute-done((bf16[512,1408]{1,0:T(8,128)(2,1)}, bf16[512,1408]{1,0:T(8,128)(2,1)}, u32[]{:S(2)}, u32[]{:S(2)}) %collective-permute-start.1) | collective-permute-done | bytes 1441824 | tf_op jit(solution)/shard_map/ppermute | solution.py:24
  108.8 35.9 %all-gather.12.cloned.1.call-done = bf16[2048,1408]{1,0:T(8,128)(2,1)} async-done(((bf16[256,1408]{1,0:T(8,128)(2,1)}), bf16[2048,1408]{1,0:T(8,128)(2,1)}) %all-gather.12.cloned.1.call-update) | async-done | bytes 5767184 | tf_op jit(solution)/shard_map/all_gather | solution.py:47
  144.7 14.9 %fusion.2 = (bf16[1024,1408]{1,0:T(8,128)(2,1)}, bf16[1024,1408]{1,0:T(8,128)(2,1)}) fusion(bf16[512,1408]{1,0:T(8,128)(2,1)} %collective-permute-done.1, bf16[512,1408]{1,0:T(8,128)(2,1)S(1)} %get-tuple-element.12, bf16[512,1408]{1,0:T(8,128)(2,1)} %collective-permute-done.2, bf16[512,1408]{1,0:T(8,128)(2,1)S(1)} %copy-done.8, ...), kind=kOutput, calls=%fused_computation.11 | convolution fusion | flops 5935857664 | bytes 21495808 | tf_op jit(solution)/shard_map/dot_general | solution.py:92
  159.6 77.7 %all-gather.16.cloned.1.call-done = bf16[2048,1408]{1,0:T(8,128)(2,1)} async-done(((bf16[256,1408]{1,0:T(8,128)(2,1)}), bf16[2048,1408]{1,0:T(8,128)(2,1)}) %all-gather.16.cloned.1.call-update) | async-done | bytes 5767184 | tf_op jit(solution)/shard_map/all_gather | solution.py:99
  237.2 11.7 %fusion.25 = f32[1024,2048]{1,0:T(8,128)} fusion(bf16[1024,1408]{1,0:T(8,128)(2,1)} %get-tuple-element.9, bf16[2048,1408]{1,0:T(8,128)(2,1)} %all-gather.16.cloned.1.call-done), kind=kOutput, calls=%fused_computation.70 | convolution fusion | flops 5905580032 | bytes 17039360 | tf_op jit(solution)/shard_map/dot_general | solution.py:18
  248.9 80.8 %all-gather.14.cloned.1.call-done = bf16[2048,1408]{1,0:T(8,128)(2,1)} async-done(((bf16[256,1408]{1,0:T(8,128)(2,1)}), bf16[2048,1408]{1,0:T(8,128)(2,1)}) %all-gather.14.cloned.1.call-update) | async-done | bytes 5767184 | tf_op jit(solution)/shard_map/all_gather | solution.py:98
  329.8 10.7 %add_convert_fusion = bf16[1024,2048]{1,0:T(8,128)(2,1)S(1)} fusion(f32[1024,2048]{1,0:T(8,128)} %fusion.25, bf16[1024,1408]{1,0:T(8,128)(2,1)S(1)} %copy-done.17, bf16[2048,1408]{1,0:T(8,128)(2,1)} %all-gather.14.cloned.1.call-done), kind=kOutput, calls=%fused_computation.3 | convolution fusion | flops 5909774336 | bytes 21233664 | tf_op jit(solution)/shard_map/dot_general | solution.py:18
  344.1 10.2 %reduce-scatter.8.cloned.1.call-done = bf16[256,2048]{1,0:T(8,128)(2,1)} async-done(((bf16[512,2048]{1,0:T(8,128)(2,1)}), bf16[256,2048]{1,0:T(8,128)(2,1)}) %reduce-scatter.8.cloned.1.call-update) | async-done | bytes 1048592 | tf_op jit(solution)/shard_map/reduce_scatter | solution.py:104
  355.5 12.7 %reduce-scatter.6.cloned.1.call-done = bf16[256,2048]{1,0:T(8,128)(2,1)} async-done(((bf16[512,2048]{1,0:T(8,128)(2,1)}), bf16[256,2048]{1,0:T(8,128)(2,1)}) %reduce-scatter.6.cloned.1.call-update) | async-done | bytes 1048592 | tf_op jit(solution)/shard_map/reduce_scatter | solution.py:104
  368.2 10.7 %collective-permute-done.3 = bf16[256,2048]{1,0:T(8,128)(2,1)S(1)} collective-permute-done((bf16[256,2048]{1,0:T(8,128)(2,1)}, bf16[256,2048]{1,0:T(8,128)(2,1)S(1)}, u32[]{:S(2)}, u32[]{:S(2)}) %collective-permute-start.3) | collective-permute-done | bytes 1048608 | tf_op jit(solution)/shard_map/ppermute | solution.py:24
  384.6 22.5 %collective-permute-done.4 = bf16[256,2048]{1,0:T(8,128)(2,1)S(1)} collective-permute-done((bf16[256,2048]{1,0:T(8,128)(2,1)}, bf16[256,2048]{1,0:T(8,128)(2,1)S(1)}, u32[]{:S(2)}, u32[]{:S(2)}) %collective-permute-start.4) | collective-permute-done | bytes 1048608 | tf_op jit(solution)/shard_map/ppermute | solution.py:24
  408.1 12.1 %convolution_convert_fusion = bf16[2048,1408]{1,0:T(8,128)(2,1)} fusion(bf16[1024,2048]{1,0:T(8,128)(2,1)} %constant_dynamic-update-slice_fusion, bf16[512,1408]{1,0:T(8,128)(2,1)} %collective-permute-done.1, bf16[512,1408]{1,0:T(8,128)(2,1)} %copy-done.9, bf16[512,1408]{1,0:T(8,128)(2,1)} %collective-permute-done.2, bf16[512,1408]{1,0:T(8,128)(2,1)} %get-tuple-element.14), kind=kOutput, calls=%fused_computation.4 | convolution fusion | flops 5928648704 | bytes 15728640 | tf_op jit(solution)/shard_map/dot_general | solution.py:12
  423.5 3.4 constant_dynamic-update-slice_fusion.2
  426.9 10.9 %convolution_convert_fusion.1 = bf16[2048,1408]{1,0:T(8,128)(2,1)} fusion(bf16[1024,2048]{1,0:T(8,128)(2,1)} %constant_dynamic-update-slice_fusion.2, bf16[1024,1408]{1,0:T(8,128)(2,1)S(1)} %copy-done.16), kind=kOutput, calls=%fused_computation.5 | convolution fusion | flops 5908463616 | bytes 12845056 | tf_op jit(solution)/shard_map/dot_general | solution.py:12
  439.7 10.9 %convolution_convert_fusion.2 = bf16[2048,1408]{1,0:T(8,128)(2,1)} fusion(bf16[1024,2048]{1,0:T(8,128)(2,1)} %constant_dynamic-update-slice_fusion.2, bf16[1024,1408]{1,0:T(8,128)(2,1)S(1)} %copy-done.18), kind=kOutput, calls=%fused_computation.6 | convolution fusion | flops 5908463616 | bytes 12845056 | tf_op jit(solution)/shard_map/dot_general | solution.py:12
  450.6 85.2 %reduce-scatter.14.cloned.1.call-done = bf16[256,1408]{1,0:T(8,128)(2,1)} async-done(((bf16[2048,1408]{1,0:T(8,128)(2,1)}), bf16[256,1408]{1,0:T(8,128)(2,1)}) %reduce-scatter.14.cloned.1.call-update) | async-done | bytes 720912 | tf_op jit(solution)/shard_map/reduce_scatter | solution.py:80
  539.9 12.5 %collective-permute-done.7 = bf16[256,1408]{1,0:T(8,128)(2,1)S(1)} collective-permute-done((bf16[256,1408]{1,0:T(8,128)(2,1)}, bf16[256,1408]{1,0:T(8,128)(2,1)S(1)}, u32[]{:S(2)}, u32[]{:S(2)}) %collective-permute-start.7) | collective-permute-done | bytes 720928 | tf_op jit(solution)/shard_map/ppermute | solution.py:24
  553.6 95.8 %reduce-scatter.12.cloned.1.call-done = bf16[256,1408]{1,0:T(8,128)(2,1)} async-done(((bf16[2048,1408]{1,0:T(8,128)(2,1)}), bf16[256,1408]{1,0:T(8,128)(2,1)}) %reduce-scatter.12.cloned.1.call-update) | async-done | bytes 720912 | tf_op jit(solution)/shard_map/reduce_scatter | solution.py:80
  653.5 109.3 %reduce-scatter.10.cloned.1.call-done = bf16[256,1408]{1,0:T(8,128)(2,1)} async-done(((bf16[2048,1408]{1,0:T(8,128)(2,1)}), bf16[256,1408]{1,0:T(8,128)(2,1)}) %reduce-scatter.10.cloned.1.call-update) | async-done | bytes 720912 | tf_op jit(solution)/shard_map/reduce_scatter | solution.py:80
  765.5 13.8 %collective-permute-done.5 = bf16[256,1408]{1,0:T(8,128)(2,1)S(1)} collective-permute-done((bf16[256,1408]{1,0:T(8,128)(2,1)}, bf16[256,1408]{1,0:T(8,128)(2,1)S(1)}, u32[]{:S(2)}, u32[]{:S(2)}) %collective-permute-start.5) | collective-permute-done | bytes 720928 | tf_op jit(solution)/shard_map/ppermute | solution.py:24
  (99 shorter events, 49.6 us)
Async XLA Ops:
  7.2 42.5 %all-gather.8.cloned.1.call-start = ((), (), s32[]{:S(2)}) async-start(), calls=%async_computation.5 | async-start | bytes 3145728 | tf_op jit(solution)/shard_map/all_gather | solution.py:69
  13.3 39.9 %all-gather.10.cloned.1.call-start = ((), (), s32[]{:S(2)}) async-start(), calls=%async_computation.6 | async-start | bytes 3145728 | tf_op jit(solution)/shard_map/all_gather | solution.py:69
  13.3 24.3 %collective-permute-start = (bf16[256,2048]{1,0:T(8,128)(2,1)}, bf16[256,2048]{1,0:T(8,128)(2,1)S(1)}, u32[]{:S(2)}, u32[]{:S(2)}) collective-permute-start(bf16[256,2048]{1,0:T(8,128)(2,1)} %fusion.11), channel_id=1, source_target_pairs={{0,16},{16,0},{1,17},{17,1},{2,18},{18,2},{3,19},{19,3},{4,20},{20... | collective-permute-start | bytes 3145736 | tf_op jit(solution)/shard_map/ppermute | solution.py:24
  38.6 106.1 %all-gather.12.cloned.1.call-start = ((), (), s32[]{:S(2)}) async-start(), calls=%async_computation.7 | async-start | bytes 6488064 | tf_op jit(solution)/shard_map/all_gather | solution.py:47
  39.6 197.6 %all-gather.16.cloned.1.call-start = ((), (), s32[]{:S(2)}) async-start(), calls=%async_computation.9 | async-start | bytes 6488064 | tf_op jit(solution)/shard_map/all_gather | solution.py:99
  41.9 287.9 %all-gather.14.cloned.1.call-start = ((), (), s32[]{:S(2)}) async-start(), calls=%async_computation.8 | async-start | bytes 6488064 | tf_op jit(solution)/shard_map/all_gather | solution.py:98
  44.1 310.3 %reduce-scatter.8.cloned.1.call-start = ((), (), s32[]{:S(2)}) async-start(), calls=%async_computation.11 | async-start | bytes 3145728 | tf_op jit(solution)/shard_map/reduce_scatter | solution.py:104
  45.9 31.9 %collective-permute-start.2 = (bf16[512,1408]{1,0:T(8,128)(2,1)}, bf16[512,1408]{1,0:T(8,128)(2,1)}, u32[]{:S(2)}, u32[]{:S(2)}) collective-permute-start(bf16[512,1408]{1,0:T(8,128)(2,1)} %get-tuple-element.15), channel_id=1, source_target_pairs={{0,16},{16,0},{1,17},{17,1},{2,18},{18,2},{3,19},{19,3},{4,20},{20... | collective-permute-start | bytes 4325384 | tf_op jit(solution)/shard_map/ppermute | solution.py:24
  48.6 96.0 %copy-start.9 = (bf16[512,1408]{1,0:T(8,128)(2,1)}, bf16[512,1408]{1,0:T(8,128)(2,1)S(1)}, u32[]{:S(2)}) copy-start(bf16[512,1408]{1,0:T(8,128)(2,1)S(1)} %get-tuple-element.12) | copy-start | bytes 4325380
  48.6 60.1 %collective-permute-start.1 = (bf16[512,1408]{1,0:T(8,128)(2,1)}, bf16[512,1408]{1,0:T(8,128)(2,1)}, u32[]{:S(2)}, u32[]{:S(2)}) collective-permute-start(bf16[512,1408]{1,0:T(8,128)(2,1)} %get-tuple-element.13), channel_id=1, source_target_pairs={{0,16},{16,0},{1,17},{17,1},{2,18},{18,2},{3,19},{19,3},{4,20},{20... | collective-permute-start | bytes 4325384 | tf_op jit(solution)/shard_map/ppermute | solution.py:24
  53.2 91.5 %copy-start.8 = (bf16[512,1408]{1,0:T(8,128)(2,1)S(1)}, bf16[512,1408]{1,0:T(8,128)(2,1)}, u32[]{:S(2)}) copy-start(bf16[512,1408]{1,0:T(8,128)(2,1)} %get-tuple-element.14) | copy-start | bytes 4325380
  237.2 92.6 %copy-start.17 = (bf16[1024,1408]{1,0:T(8,128)(2,1)S(1)}, bf16[1024,1408]{1,0:T(8,128)(2,1)}, u32[]{:S(2)}) copy-start(bf16[1024,1408]{1,0:T(8,128)(2,1)} %get-tuple-element.8) | copy-start | bytes 8650756
  343.1 37.8 %copy-start.2 = (bf16[256,2048]{1,0:T(8,128)(2,1)S(1)}, bf16[256,2048]{1,0:T(8,128)(2,1)}, u32[]{:S(2)}) copy-start(bf16[256,2048]{1,0:T(8,128)(2,1)} %param.16) | copy-start | bytes 3145732
  343.1 25.1 %reduce-scatter.6.cloned.1.call-start = ((), (), s32[]{:S(2)}) async-start(), calls=%async_computation.10 | async-start | bytes 3145728 | tf_op jit(solution)/shard_map/reduce_scatter | solution.py:104
  343.9 76.5 %all-gather.18.cloned.1.call-start = ((), (), s32[]{:S(2)}) async-start(), calls=%async_computation.12 | async-start | bytes 3145728 | tf_op jit(solution)/shard_map/all_gather | solution.py:68
  354.3 24.6 %collective-permute-start.3 = (bf16[256,2048]{1,0:T(8,128)(2,1)}, bf16[256,2048]{1,0:T(8,128)(2,1)S(1)}, u32[]{:S(2)}, u32[]{:S(2)}) collective-permute-start(bf16[256,2048]{1,0:T(8,128)(2,1)} %reduce-scatter.8.cloned.1.call-done), channel_id=1, source_target_pairs={{0,16},{16,0},{1,17},{17,1},{2,18},{18,2},{3,19},{19,3},{4,20},{20... | collective-permute-start | bytes 3145736 | tf_op jit(solution)/shard_map/ppermute | solution.py:24
  383.2 40.3 %all-gather.20.cloned.1.call-start = ((), (), s32[]{:S(2)}) async-start(), calls=%async_computation.13 | async-start | bytes 3145728 | tf_op jit(solution)/shard_map/all_gather | solution.py:68
  383.3 23.8 %collective-permute-start.4 = (bf16[256,2048]{1,0:T(8,128)(2,1)}, bf16[256,2048]{1,0:T(8,128)(2,1)S(1)}, u32[]{:S(2)}, u32[]{:S(2)}) collective-permute-start(bf16[256,2048]{1,0:T(8,128)(2,1)} %get-tuple-element.16), channel_id=1, source_target_pairs={{0,16},{16,0},{1,17},{17,1},{2,18},{18,2},{3,19},{19,3},{4,20},{20... | collective-permute-start | bytes 3145736 | tf_op jit(solution)/shard_map/ppermute | solution.py:24
  408.1 127.6 %reduce-scatter.14.cloned.1.call-start = ((), (), s32[]{:S(2)}) async-start(), calls=%async_computation.16 | async-start | bytes 6488064 | tf_op jit(solution)/shard_map/reduce_scatter | solution.py:80
  420.3 229.0 %reduce-scatter.12.cloned.1.call-start = ((), (), s32[]{:S(2)}) async-start(), calls=%async_computation.15 | async-start | bytes 6488064 | tf_op jit(solution)/shard_map/reduce_scatter | solution.py:80
  437.8 325.0 %reduce-scatter.10.cloned.1.call-start = ((), (), s32[]{:S(2)}) async-start(), calls=%async_computation.14 | async-start | bytes 6488064 | tf_op jit(solution)/shard_map/reduce_scatter | solution.py:80
  535.7 16.6 %collective-permute-start.7 = (bf16[256,1408]{1,0:T(8,128)(2,1)}, bf16[256,1408]{1,0:T(8,128)(2,1)S(1)}, u32[]{:S(2)}, u32[]{:S(2)}) collective-permute-start(bf16[256,1408]{1,0:T(8,128)(2,1)} %reduce-scatter.14.cloned.1.call-done), channel_id=1, source_target_pairs={{0,16},{16,0},{1,17},{17,1},{2,18},{18,2},{3,19},{19,3},{4,20},{20... | collective-permute-start | bytes 2162696 | tf_op jit(solution)/shard_map/ppermute | solution.py:24
  649.3 115.0 %collective-permute-start.6 = (bf16[256,1408]{1,0:T(8,128)(2,1)}, bf16[256,1408]{1,0:T(8,128)(2,1)S(1)}, u32[]{:S(2)}, u32[]{:S(2)}) collective-permute-start(bf16[256,1408]{1,0:T(8,128)(2,1)} %reduce-scatter.12.cloned.1.call-done), channel_id=1, source_target_pairs={{0,16},{16,0},{1,17},{17,1},{2,18},{18,2},{3,19},{19,3},{4,20},{20... | collective-permute-start | bytes 2162696 | tf_op jit(solution)/shard_map/ppermute | solution.py:24
  762.8 16.5 %collective-permute-start.5 = (bf16[256,1408]{1,0:T(8,128)(2,1)}, bf16[256,1408]{1,0:T(8,128)(2,1)S(1)}, u32[]{:S(2)}, u32[]{:S(2)}) collective-permute-start(bf16[256,1408]{1,0:T(8,128)(2,1)} %reduce-scatter.10.cloned.1.call-done), channel_id=1, source_target_pairs={{0,16},{16,0},{1,17},{17,1},{2,18},{18,2},{3,19},{19,3},{4,20},{20... | collective-permute-start | bytes 2162696 | tf_op jit(solution)/shard_map/ppermute | solution.py:24
  (15 other events, 156.6 us)
Sparse Core Ops, SparseCore 0:
  13.4 12.4 all-gather.7
  38.7 13.3 all-gather.9
  54.3 90.3 all-gather.11
  146.7 90.4 all-gather.15
  239.3 90.4 all-gather.13
  343.2 11.0 reduce-scatter.7
  357.1 11.0 reduce-scatter.5
  383.4 12.7 all-gather.17
  408.2 13.5 all-gather.19
  425.3 110.3 reduce-scatter.13
  539.4 109.9 reduce-scatter.11
  652.8 109.9 reduce-scatter.9
where the time goes:
time: 791 us; the launch traced here: 788 us
  waiting for transfers between devices  643 us (81%)
  matrix products  71.2 us (9%)
  local copies, waits for them, and re-layouts  33 us (4%)
  other arithmetic  15.3 us (2%)
  between operations  14.4 us (2%)
  starting transfers between devices  10.6 us (1%)
    reduce_scatter x3, waiting for transfers between devices, spread(): lax.psum_scatter(total.astype(bf16), 'fs', scatter_dimension=0, tiled=True)  290 us
    ppermute x8, waiting for transfers between devices, shifted(): lax.ppermute(value, 'rep', [(i, (i + step) % reps) for i in range(reps)])  135 us
    all_gather x1, waiting for transfers between devices, per_device(): lax.all_gather(columns(gate_weight, me), 'fs', axis=0, tiled=True)  80.8 us
    all_gather x1, waiting for transfers between devices, per_device(): up_full = lax.all_gather(columns(up_weight, me), 'fs', axis=0, tiled=True)  77.7 us
    all_gather x1, waiting for transfers between devices, per_device(): lax.all_gather(columns(down_weight, me), 'fs', axis=0, tiled=True)  35.9 us
    dot_general x3, matrix products, contract_rows(): lax.dot_general(left, right, (((0,), (0,)), ((), ())), preferred_element_...  33.9 us
    reduce_scatter x2, waiting for transfers between devices, per_device(): lax.psum_scatter(partial[k * rows:(k + 1) * rows], 'tp', scatter_dimensio...  22.9 us
    dot_general x2, matrix products, contract_cols(): lax.dot_general(left, right, (((1,), (1,)), ((), ())), preferred_element_...  22.4 us
  transfers between devices with their start and end apart: 20, of which 15 were waited for; matrix products, arithmetic and copies ran while one was open for 12% of the time, Pallas kernels for 0%

commit v1 on v0

--- a/solution.py
+++ b/solution.py
@@ -3,9 +3,13 @@
 import jax
 import jax.numpy as jnp
 from jax import lax
+from jax.experimental import pallas as pl
+from jax.experimental.pallas import tpu as pltpu
 from jax.sharding import PartitionSpec as P
 
 eps = 1e-06
+bf16, f32 = jnp.bfloat16, jnp.float32
+SEMS, LOCALS = 200, 64
 
 
 def contract_rows(left, right):
@@ -24,7 +28,7 @@
     return lax.ppermute(value, "rep", [(i, (i + step) % reps) for i in range(reps)])
 
 
-def per_device(
+def plain_device(
     reps,
     block_input,
     pre_gain,
@@ -37,7 +41,6 @@
     up_weight,
     down_weight,
 ):
-    bf16, f32 = jnp.bfloat16, jnp.float32
     me = lax.axis_index("rep")
     width = gate_saved.shape[1] // reps
 
@@ -118,22 +121,718 @@
     return (input_grad.astype(bf16), gate_grad, up_grad, down_grad)
 
 
+LANE = 128
+MESH = pl.DeviceIdType.MESH
+
+
+class Links:
+    def __init__(self, send, recv, local):
+        self.send, self.recv, self.local = send, recv, local
+        self.names, self.count, self.pending, self.locals = {}, 0, [], 0
+
+    def index(self, name, size=1):
+        if name not in self.names:
+            self.names[name] = self.count
+            self.count += size
+        return self.names[name]
+
+    def make(self, name, src, dst, device, size=1, send_at=0, recv_at=0):
+        base = self.index(name, size)
+        return pltpu.make_async_remote_copy(
+            src_ref=src,
+            dst_ref=dst,
+            send_sem=self.send.at[base + send_at],
+            recv_sem=self.recv.at[base + recv_at],
+            device_id=device,
+            device_id_type=MESH,
+        )
+
+    def start(self, name, src, dst, device, when=None, **at):
+        copy = self.make(name, src, dst, device, **at)
+        guarded(when, copy.start)
+        self.pending.append((when, copy))
+
+    def arrive(self, name, dst, device, when=None, **at):
+        guarded(when, self.make(name, dst, dst, device, **at).wait_recv)
+
+    def here(self, src, dst, when=None):
+        copy = pltpu.make_async_copy(src, dst, self.local.at[self.locals])
+        self.locals += 1
+        guarded(when, copy.start)
+        return lambda: guarded(when, copy.wait)
+
+    def finish(self):
+        for when, copy in self.pending:
+            guarded(when, copy.wait_send)
+
+
+def guarded(when, action):
+    if when is None:
+        action()
+    else:
+        pl.when(when)(action)
+
+
+def fused_kernel(
+    nz,
+    normed,
+    branch,
+    gate,
+    up,
+    down_w,
+    gate_w,
+    up_w,
+    down_out,
+    gate_out,
+    up_out,
+    sum_own,
+    sum_far,
+    rows,
+    acts,
+    weights,
+    parts,
+    halves,
+    near,
+    mate,
+    side,
+    tile,
+    send,
+    recv,
+    local,
+):
+    x, f, c = (lax.axis_index(a) for a in ("rep", "fs", "tp"))
+    y, z = lax.rem(f, 2), lax.div(f, 2)
+    links = Links(send, recv, local)
+    to_x = {"rep": 1 - x}
+    to_y = {"fs": f + 1 - 2 * y}
+    to_d = {"rep": 1 - x, "fs": f + 1 - 2 * y}
+    to_c = {"tp": 1 - c}
+    to_up, to_dn = {"fs": f + 2}, {"fs": f - 2}
+    has_up, has_dn = z < nz - 1, z > 0
+
+    tokens, model = normed.shape
+    chip = gate.shape[0]
+    feats = down_w.shape[0]
+    block = 2 * feats
+    half = gate.shape[1] // 2
+    full = acts.shape[2]
+    main = full - LANE
+    cut = full // 2
+    wide, slim = y == c, y != c
+    sources = (down_w, gate_w, up_w)
+    outs = (down_out, gate_out, up_out)
+
+    def lanes(start, size):
+        return pl.ds(pl.multiple_of(start, LANE), size)
+
+    barrier = pltpu.get_barrier_semaphore()
+    for device in (to_x, to_y, to_d, to_c):
+        pl.semaphore_signal(barrier, inc=1, device_id=device, device_id_type=MESH)
+
+    @pl.when(has_up)
+    def _():
+        pl.semaphore_signal(barrier, inc=1, device_id=to_up, device_id_type=MESH)
+
+    @pl.when(has_dn)
+    def _():
+        pl.semaphore_signal(barrier, inc=1, device_id=to_dn, device_id_type=MESH)
+
+    def own_cols(xx, yy, lo, hi):
+        return lanes(xx * half + yy * (main + LANE) + lo, hi - lo)
+
+    def extra_cols(xx):
+        return lanes(xx * half + main, LANE)
+
+    my_feats = pl.ds(f * feats, feats)
+    own_weight = []
+    for w in range(3):
+        own_weight.append(
+            (
+                links.here(
+                    sources[w].at[:, own_cols(x, y, 0, main)],
+                    weights.at[w, my_feats, pl.ds(0, main)],
+                ),
+                links.here(
+                    sources[w].at[:, extra_cols(x)],
+                    weights.at[w, my_feats, pl.ds(main, LANE)],
+                    wide,
+                ),
+            )
+        )
+    own_acts = []
+    for g, saved in ((1, gate), (2, up)):
+        own_acts.append(
+            links.here(saved.at[:, own_cols(x, y, 0, main)], acts.at[g, pl.ds(0, chip), pl.ds(0, main)])
+        )
+        own_acts.append(
+            links.here(
+                saved.at[:, extra_cols(x)], acts.at[g, pl.ds(0, chip), pl.ds(main, LANE)], wide
+            )
+        )
+
+    def slot_rows(slot, core):
+        return pl.ds((slot * 2 + core) * tokens, tokens)
+
+    own_rows = [
+        links.here(branch, rows.at[0, slot_rows(0, c), :]),
+        links.here(normed, rows.at[1, slot_rows(0, c), :]),
+    ]
+
+    pl.semaphore_wait(barrier, 4 + has_up.astype(jnp.int32) + has_dn.astype(jnp.int32))
+
+    tables = (branch, normed)
+    part = model // 2
+
+    def row_cols(h):
+        return pl.ds(h * part, part)
+
+    def row_send(a, kind):
+        h = 0 if kind in ("y1", "x2", "x3") else 1
+        device = to_y if kind[0] == "y" else to_x
+        if kind in ("x3", "y3"):
+            source = rows.at[a, slot_rows(1 if kind == "x3" else 2, c), row_cols(h)]
+            target = 3
+        else:
+            source = tables[a].at[:, row_cols(h)]
+            target = 1 if kind[0] == "y" else 2
+        links.start(f"r{a}{kind}", source, rows.at[a, slot_rows(target, c), row_cols(h)], device)
+
+    def row_wait(a, kind):
+        h = 0 if kind in ("y1", "x2", "x3") else 1
+        device = to_y if kind[0] == "y" else to_x
+        target = 3 if kind in ("x3", "y3") else (1 if kind[0] == "y" else 2)
+        links.arrive(f"r{a}{kind}", rows.at[a, slot_rows(target, c), row_cols(h)], device)
+
+    def mate_send(a, slot):
+        where = rows.at[a, slot_rows(slot, c), :]
+        source = tables[a] if slot == 0 else where
+        links.start(f"m{a}{slot}", source, where, to_c)
+
+    def mate_wait(a, slot):
+        links.arrive(f"m{a}{slot}", rows.at[a, slot_rows(slot, 1 - c), :], to_c)
+
+    def y_weight(w):
+        there = weights.at[w, my_feats, :]
+        links.start(
+            f"w{w}y",
+            sources[w].at[:, own_cols(x, 1 - y, 0, main)],
+            there.at[:, pl.ds(0, main)],
+            to_y,
+        )
+        links.start(
+            f"w{w}e", sources[w].at[:, extra_cols(x)], there.at[:, pl.ds(main, LANE)], to_y, slim
+        )
+
+    def y_weight_wait(w):
+        there = weights.at[w, pl.ds((f + 1 - 2 * y) * feats, feats), :]
+        links.arrive(f"w{w}y", there.at[:, pl.ds(0, main)], to_y)
+        links.arrive(f"w{w}e", there.at[:, pl.ds(main, LANE)], to_y, wide)
+
+    def weight_piece(w, origin, o, width):
+        yy = y if o == 0 else 1 - y
+        return weights.at[w, pl.ds((origin * 2 + yy) * feats, feats), pl.ds(0, width)]
+
+    def z_send(w, o, hop):
+        for width, size in ((full, wide), (main, slim)):
+            ahead = weight_piece(w, jnp.maximum(z - hop, 0), o, width)
+            when = size & has_up & (z >= hop)
+            links.start(f"z{w}{o}u{hop}", ahead, ahead, to_up, when)
+            behind = weight_piece(w, jnp.minimum(z + hop, nz - 1), o, width)
+            when = size & has_dn & (z + hop < nz)
+            links.start(f"z{w}{o}d{hop}", behind, behind, to_dn, when)
+
+    def z_wait(w, o, hop):
+        for width, size in ((full, wide), (main, slim)):
+            ahead = weight_piece(w, jnp.maximum(z - hop, 0), o, width)
+            links.arrive(f"z{w}{o}u{hop - 1}", ahead, to_up, size & (z >= hop))
+            behind = weight_piece(w, jnp.minimum(z + hop, nz - 1), o, width)
+            links.arrive(f"z{w}{o}d{hop - 1}", behind, to_dn, size & (z + hop < nz))
+
+    def z_step(w, o, hop):
+        z_wait(w, o, hop)
+        if hop < nz - 1:
+            z_send(w, o, hop)
+
+    peers = ((2, to_x, 1 - x, y), (1, to_y, x, 1 - y), (3, to_d, 1 - x, 1 - y))
+
+    def act_send(q):
+        for slot, device, xx, yy in peers:
+            for g, saved in ((1, gate), (2, up)):
+                there = acts.at[g, pl.ds(slot * chip, chip), :]
+                lo, hi = (0, cut) if q == 0 else (cut, main)
+                links.start(
+                    f"a{q}{g}{slot}",
+                    saved.at[:, own_cols(xx, yy, lo, hi)],
+                    there.at[:, pl.ds(lo, hi - lo)],
+                    device,
+                )
+                if q == 1:
+                    links.start(
+                        f"e{g}{slot}",
+                        saved.at[:, extra_cols(xx)],
+                        there.at[:, pl.ds(main, LANE)],
+                        device,
+                        yy == c,
+                    )
+
+    def act_wait(q):
+        for slot, device, _, _ in peers:
+            for g in (1, 2):
+                there = acts.at[g, pl.ds(slot * chip, chip), :]
+                lo, hi = (0, cut) if q == 0 else (cut, main)
+                links.arrive(f"a{q}{g}{slot}", there.at[:, pl.ds(lo, hi - lo)], device)
+                if q == 1:
+                    links.arrive(f"e{g}{slot}", there.at[:, pl.ds(main, LANE)], device, wide)
+
+    total = acts.shape[1]
+
+    def make_hidden(q):
+        cols = pl.ds(q * cut, cut)
+
+        @pl.loop(0, total // 64)
+        def _(i):
+            at = pl.ds(i * 64, 64)
+            g = acts[1, at, cols].astype(f32)
+            u = acts[2, at, cols].astype(f32)
+            acts[0, at, cols] = (g * jax.nn.sigmoid(g) * u).astype(bf16)
+
+    def make_cots(q):
+        cols = pl.ds(q * cut, cut)
+
+        @pl.loop(0, total // 256)
+        def _(i):
+            at = pl.ds(i * 256, 256)
+            tile[pl.ds(0, 256), :] = jnp.dot(
+                rows[0, at, :], weights[0, :, cols], preferred_element_type=f32
+            )
+
+            @pl.loop(0, 4)
+            def _(j):
+                sub = pl.ds(i * 256 + j * 64, 64)
+                grad = tile[pl.ds(j * 64, 64), :]
+                g = acts[1, sub, cols].astype(f32)
+                u = acts[2, sub, cols].astype(f32)
+                s = jax.nn.sigmoid(g)
+                acts[1, sub, cols] = (grad * u * s * (1.0 + g * (1.0 - s))).astype(bf16)
+                acts[2, sub, cols] = (grad * (g * s)).astype(bf16)
+
+    def order(s):
+        def low(zz):
+            return jnp.where(
+                s < nz - 1 - zz, nz - 1 - s, jnp.where(s == nz - 1, zz, s - (nz - 1 - zz))
+            )
+
+        return jnp.where(2 * z < nz, low(z), nz - 1 - low(nz - 1 - z))
+
+    def grad_step(q, g, s):
+        d = order(s)
+        cols = lanes(q * cut, cut)
+
+        @pl.loop(0, block // 256)
+        def _(m):
+            tile[pl.ds(m * 256, 256), :] = contract_rows(
+                rows[jnp.minimum(g, 1), :, pl.ds(pl.multiple_of(d * block + m * 256, 256), 256)],
+                acts[g, :, cols],
+            )
+
+        sizes = ((cut, (q == 0) | wide), (cut - LANE, (q == 1) & slim))
+        spot = (q * 3 + g) * (nz + 1)
+        count = 6 * (nz + 1)
+
+        def take(slot, when):
+            for width, size in sizes:
+                links.arrive(
+                    "p",
+                    parts.at[g, slot, :, lanes(q * cut, width)],
+                    to_up,
+                    when & size,
+                    size=count,
+                    recv_at=spot + slot,
+                )
+
+        far = d != z
+        fed = jnp.where(d > z, has_dn, jnp.where(d < z, has_up, has_dn))
+        take(d, fed)
+
+        @pl.loop(0, block // 64)
+        def _(i):
+            at = pl.ds(i * 64, 64)
+
+            @pl.when(fed)
+            def _():
+                tile[at, :] += parts[g, d, at, cols].astype(f32)
+
+        take(nz, (d == z) & has_up)
+
+        @pl.when((d == z) & has_up)
+        def _():
+            @pl.loop(0, block // 64)
+            def _(i):
+                at = pl.ds(i * 64, 64)
+                tile[at, :] += parts[g, nz, at, cols].astype(f32)
+
+        @pl.loop(0, block // 64)
+        def _(i):
+            at = pl.ds(i * 64, 64)
+            parts[g, d, at, cols] = tile[at, :].astype(bf16)
+
+        target = jnp.where(d == z - 1, nz, d)
+        device = {"fs": jnp.where(d > z, f + 2, f - 2)}
+        for width, size in sizes:
+            copy = links.make(
+                "p",
+                parts.at[g, d, :, lanes(q * cut, width)],
+                parts.at[g, target, :, lanes(q * cut, width)],
+                device,
+                size=count,
+                send_at=spot + d,
+                recv_at=spot + target,
+            )
+            guarded(far & size, copy.start)
+
+    def grad_sent():
+        @pl.loop(0, 6)
+        def _(i):
+            q, g = lax.div(i, 3), lax.rem(i, 3)
+            spot = i * (nz + 1)
+
+            @pl.loop(0, nz)
+            def _(d):
+                for width, size in (
+                    (cut, (q == 0) | wide),
+                    (cut - LANE, (q == 1) & slim),
+                ):
+                    copy = links.make(
+                        "p",
+                        parts.at[g, d, :, lanes(q * cut, width)],
+                        parts.at[g, d, :, lanes(q * cut, width)],
+                        to_up,
+                        send_at=spot + d,
+                        recv_at=spot + d,
+                    )
+                    guarded((d != z) & size, copy.wait_send)
+
+    out_waits = []
+
+    def mine(g, yy, lo, hi):
+        return lanes(yy * (main + LANE) + lo, hi - lo)
+
+    def spread(q, g):
+        lo, hi = (0, cut) if q == 0 else (cut, main)
+
+        @pl.loop(0, feats // 64)
+        def _(i):
+            at = pl.ds(i * 64, 64)
+            src = pl.ds(y * feats + i * 64, 64)
+            halves[g, at, mine(g, y, lo, hi)] = parts[g, z, src, pl.ds(lo, hi - lo)]
+
+        if q == 1:
+
+            @pl.when(wide)
+            def _():
+                @pl.loop(0, feats // 64)
+                def _(i):
+                    at = pl.ds(i * 64, 64)
+                    src = pl.ds(y * feats + i * 64, 64)
+                    halves[g, at, pl.ds(main, LANE)] = parts[g, z, src, pl.ds(main, LANE)]
+
+        send_rows = parts.at[g, z, pl.ds((1 - y) * feats, feats), :]
+        links.start(
+            f"h{q}{g}y", send_rows.at[:, pl.ds(lo, hi - lo)], halves.at[g, :, mine(g, y, lo, hi)], to_y
+        )
+        if q == 1:
+            links.start(
+                f"h{g}e",
+                send_rows.at[:, pl.ds(main, LANE)],
+                halves.at[g, :, pl.ds(main, LANE)],
+                to_y,
+                wide,
+            )
+        leave(q, g, "o", mine(g, y, lo, hi), y * (main + LANE) + lo, hi - lo)
+
+    def leave(q, g, tag, cols, start, size):
+        there = outs[g].at[:, lanes(x * half + start, size)]
+        links.start(f"h{q}{g}{tag}", halves.at[g, :, cols], there, to_x)
+        out_waits.append(links.here(halves.at[g, :, cols], there))
+        back = outs[g].at[:, lanes((1 - x) * half + start, size)]
+        out_waits.append(lambda: links.arrive(f"h{q}{g}{tag}", back, to_x))
+
+    def spread_on(q, g):
+        lo, hi = (0, cut) if q == 0 else (cut, main)
+        links.arrive(f"h{q}{g}y", halves.at[g, :, mine(g, 1 - y, lo, hi)], to_y)
+        leave(q, g, "n", mine(g, 1 - y, lo, hi), (1 - y) * (main + LANE) + lo, hi - lo)
+        if q == 1:
+            links.arrive(f"h{g}e", halves.at[g, :, pl.ds(main, LANE)], to_y, slim)
+            leave(q, g, "e", pl.ds(main, LANE), main, LANE)
+
+    def row_grad(core, target, add):
+        @pl.loop(0, 16)
+        def _(i):
+            k, n = lax.div(i, 4), lax.rem(i, 4)
+            slot = lax.rem(k * 2 + 1, 4) - lax.div(k, 2)
+            at = pl.ds((slot * 2 + core) * tokens, tokens)
+            wide_cols = pl.ds(pl.multiple_of(n * (model // 4), 512), model // 4)
+            feat_rows = pl.ds(n * (model // 4), model // 4)
+            value = contract_cols(acts[1, at, :], weights[1, feat_rows, :])
+            value = value + contract_cols(acts[2, at, :], weights[2, feat_rows, :])
+            if add:
+                value = value + mate[slot, :, wide_cols].astype(f32)
+            target[slot, :, wide_cols] = value.astype(bf16)
+
+    def add_into(target, source):
+        @pl.loop(0, tokens // 32)
+        def _(i):
+            at = pl.ds(i * 32, 32)
+            target[at, :] = (target[at, :].astype(f32) + source[at, :].astype(f32)).astype(bf16)
+
+    mate_send(0, 0)
+    mate_send(1, 0)
+    y_weight(0)
+    for kind in ("y1", "x1", "x2", "y2"):
+        row_send(0, kind)
+    for wait in own_weight[0]:
+        wait()
+    z_send(0, 0, 0)
+    y_weight_wait(0)
+    z_send(0, 1, 0)
+    row_wait(0, "x1")
+    row_send(0, "y3")
+    row_wait(0, "y1")
+    row_send(0, "x3")
+    act_send(0)
+    for kind in ("y1", "x1", "x2", "y2"):
+        row_send(1, kind)
+
+    @pl.when(slim)
+    def _():
+        @pl.loop(0, total // 64)
+        def _(i):
+            at = pl.ds(i * 64, 64)
+            for g in (1, 2):
+                acts[g, at, pl.ds(main, LANE)] = jnp.zeros((64, LANE), bf16)
+
+        @pl.loop(0, model // 64)
+        def _(i):
+            at = pl.ds(i * 64, 64)
+            for w in range(3):
+                weights[w, at, pl.ds(main, LANE)] = jnp.zeros((64, LANE), bf16)
+
+    z_step(0, 0, 1)
+    z_step(0, 1, 1)
+    row_wait(0, "y2")
+    mate_send(0, 1)
+    row_wait(0, "x2")
+    mate_send(0, 2)
+    z_step(0, 0, 2)
+    z_step(0, 1, 2)
+    for w in (1, 2):
+        for wait in own_weight[w]:
+            wait()
+        z_send(w, 0, 0)
+    row_wait(0, "x3")
+    row_wait(0, "y3")
+    mate_send(0, 3)
+    z_step(0, 0, 3)
+    z_step(0, 1, 3)
+    for w in (1, 2):
+        z_step(w, 0, 1)
+    for wait in own_acts + own_rows:
+        wait()
+    act_wait(0)
+    make_hidden(0)
+    for slot in range(4):
+        mate_wait(0, slot)
+    row_wait(1, "x1")
+    row_send(1, "y3")
+    row_wait(1, "y1")
+    row_send(1, "x3")
+    y_weight(1)
+    y_weight(2)
+    act_send(1)
+
+    @pl.loop(0, 2)
+    def _(i):
+        grad_step(0, 0, i)
+
+    for w in (1, 2):
+        z_step(w, 0, 2)
+    make_cots(0)
+
+    @pl.loop(2, 4)
+    def _(i):
+        grad_step(0, 0, i)
+
+    spread(0, 0)
+    row_wait(1, "y2")
+    mate_send(1, 1)
+    row_wait(1, "x2")
+    mate_send(1, 2)
+    row_wait(1, "x3")
+    row_wait(1, "y3")
+    mate_send(1, 3)
+    for w in (1, 2):
+        z_step(w, 0, 3)
+    for slot in range(4):
+        mate_wait(1, slot)
+
+    @pl.loop(0, 4)
+    def _(i):
+        grad_step(0, 1 + lax.rem(i, 2), lax.div(i, 2))
+
+    spread_on(0, 0)
+    for w in (1, 2):
+        y_weight_wait(w)
+        z_send(w, 1, 0)
+    act_wait(1)
+    make_hidden(1)
+
+    @pl.loop(0, 1)
+    def _(i):
+        grad_step(1, 0, i)
+
+    make_cots(1)
+
+    @pl.loop(4, 8)
+    def _(i):
+        grad_step(0, 1 + lax.rem(i, 2), lax.div(i, 2))
+
+    spread(0, 1)
+    spread(0, 2)
+    for w in (1, 2):
+        z_step(w, 1, 1)
+
+    @pl.loop(1, 6)
+    def _(i):
+        grad_step(1, lax.rem(i, 3), lax.div(i, 3))
+
+    spread_on(0, 1)
+    spread_on(0, 2)
+    for w in (1, 2):
+        z_step(w, 1, 2)
+    for w in (1, 2):
+        z_step(w, 1, 3)
+    row_grad(1 - c, near, False)
+    for slot in range(4):
+        links.start(f"s{slot}", near.at[slot], mate.at[slot], to_c)
+
+    @pl.loop(6, 9)
+    def _(i):
+        grad_step(1, lax.rem(i, 3), lax.div(i, 3))
+
+    for slot in range(4):
+        links.arrive(f"s{slot}", mate.at[slot], to_c)
+    row_grad(c, mate, True)
+    for i in range(2):
+        links.start(f"t{i}", mate.at[2 * i + 1], side.at[i], to_y)
+
+    @pl.loop(9, 12)
+    def _(i):
+        grad_step(1, lax.rem(i, 3), lax.div(i, 3))
+
+    for g in range(3):
+        spread(1, g)
+    links.arrive("t1", side.at[1], to_y)
+    add_into(mate.at[2], side.at[1])
+    links.start("t2", mate.at[2], sum_far, to_x)
+    links.arrive("t0", side.at[0], to_y)
+    add_into(mate.at[0], side.at[0])
+    out_waits.append(links.here(mate.at[0], sum_own))
+    for g in range(3):
+        spread_on(1, g)
+    links.arrive("t2", sum_far, to_x)
+    for wait in out_waits:
+        wait()
+    grad_sent()
+    links.finish()
+
+
+def fused_device(nz, block_input, pre_gain, post_gain, gate_saved, up_saved, branch_saved,
+                 out_cotangent, gate_weight, up_weight, down_weight):
+    xfull = block_input.astype(f32)
+    inv_x = lax.rsqrt(jnp.mean(xfull * xfull, axis=-1, keepdims=True) + eps)
+    normed = (xfull * inv_x * pre_gain).astype(bf16)
+    branch = branch_saved.astype(f32)
+    inv_b = lax.rsqrt(jnp.mean(branch * branch, axis=-1, keepdims=True) + eps)
+    upstream = 0.5 * out_cotangent.astype(f32) * post_gain
+    branch_grad = (
+        inv_b * upstream - branch * inv_b**3 * jnp.mean(upstream * branch, axis=-1, keepdims=True)
+    ).astype(bf16)
+
+    tokens, model = block_input.shape
+    chip, width = gate_saved.shape
+    feats = down_weight.shape[0]
+    half = width // 2
+    full = (half // LANE + 1) // 2 * LANE
+    grad = jax.ShapeDtypeStruct((feats, width), bf16)
+    total = jax.ShapeDtypeStruct((tokens, model), bf16)
+    down_grad, gate_grad, up_grad, sum_own, sum_far = pl.pallas_call(
+        functools.partial(fused_kernel, nz),
+        out_shape=(grad, grad, grad, total, total),
+        in_specs=[pl.BlockSpec(memory_space=pl.ANY)] * 7,
+        out_specs=[pl.BlockSpec(memory_space=pl.ANY)] * 5,
+        scratch_shapes=[
+            pltpu.VMEM((2, 4 * chip, model), bf16),
+            pltpu.VMEM((3, 4 * chip, full), bf16),
+            pltpu.VMEM((3, model, full), bf16),
+            pltpu.VMEM((3, nz + 1, 2 * feats, full), bf16),
+            pltpu.VMEM((3, feats, half), bf16),
+            pltpu.VMEM((4, tokens, model), bf16),
+            pltpu.VMEM((4, tokens, model), bf16),
+            pltpu.VMEM((2, tokens, model), bf16),
+            pltpu.VMEM((2 * feats, full // 2), f32),
+            pltpu.SemaphoreType.DMA((SEMS,)),
+            pltpu.SemaphoreType.DMA((SEMS,)),
+            pltpu.SemaphoreType.DMA((LOCALS,)),
+        ],
+        compiler_params=pltpu.CompilerParams(
+            collective_id=0, has_side_effects=True, vmem_limit_bytes=66_900_000
+        ),
+    )(normed, branch_grad, gate_saved, up_saved, down_weight, gate_weight, up_weight)
+
+    normed_grad = sum_own.astype(f32) + sum_far.astype(f32)
+    scaled = normed_grad * pre_gain
+    input_grad = (
+        out_cotangent.astype(f32)
+        + inv_x * scaled
+        - xfull * inv_x**3 * jnp.mean(scaled * xfull, axis=-1, keepdims=True)
+    )
+    return (
+        input_grad.astype(bf16),
+        gate_grad.astype(f32),
+        up_grad.astype(f32),
+        down_grad.astype(f32),
+    )
+
+
 def solution(mesh):
-    return jax.shard_map(
-        functools.partial(per_device, mesh.shape["rep"]),
-        mesh=mesh,
-        in_specs=(
-            P(("rep", "fs", "tp"), None),
-            P(),
-            P(),
-            P(("rep", "fs"), "tp"),
-            P(("rep", "fs"), "tp"),
-            P(("rep", "fs", "tp"), None),
-            P(("rep", "fs", "tp"), None),
-            P("fs", "tp"),
-            P("fs", "tp"),
-            P("fs", "tp"),
-        ),
-        out_specs=(P(("rep", "fs", "tp"), None), P("fs", "tp"), P("fs", "tp"), P("fs", "tp")),
-        check_vma=False,
-    )
+    shape = mesh.shape
+
+    def run(*args):
+        width = args[3].shape[1] // shape["tp"]
+        tiles, odd = divmod(width // 2, LANE)
+        fits = shape["rep"] == 2 and shape["tp"] == 2 and shape["fs"] % 2 == 0
+        fits = fits and width % 2 == 0 and odd == 0 and tiles % 4 == 3
+        if fits:
+            per_device = functools.partial(fused_device, shape["fs"] // 2)
+        else:
+            per_device = functools.partial(plain_device, shape["rep"])
+        return jax.shard_map(
+            per_device,
+            mesh=mesh,
+            in_specs=(
+                P(("rep", "fs", "tp"), None),
+                P(),
+                P(),
+                P(("rep", "fs"), "tp"),
+                P(("rep", "fs"), "tp"),
+                P(("rep", "fs", "tp"), None),
+                P(("rep", "fs", "tp"), None),
+                P("fs", "tp"),
+                P("fs", "tp"),
+                P("fs", "tp"),
+            ),
+            out_specs=(P(("rep", "fs", "tp"), None), P("fs", "tp"), P("fs", "tp"), P("fs", "tp")),
+            check_vma=False,
+        )(*args)
+
+    return run

time: 791 us -> 409 us (0.52)
  waiting for transfers between devices: 643 us -> 0 us
  Pallas kernels: 0 us -> 390 us
  matrix products: 71.2 us -> 0 us
  local copies, waits for them, and re-layouts: 33 us -> 0.54 us
  between operations: 14.4 us -> 0.74 us
  starting transfers between devices: 10.6 us -> 0 us
    pallas_call x0 -> x1, Pallas kernels: none -> 390 us  [fused_device(): pl.pallas_call(functools.partial(fused_kernel, nz), out_shape=(grad, grad...]
    reduce_scatter x5 -> x0, waiting for transfers between devices: 313 us -> none  [the longest x3 290 us: spread(): lax.psum_scatter(total.astype(bf16), 'fs', scatter_dimension=0, tiled=True)]
    all_gather x7 -> x0, waiting for transfers between devices: 194 us -> none  [the longest x1 80.8 us: per_device(): lax.all_gather(columns(gate_weight, me), 'fs', axis=0, tiled=True)]
    ppermute x8 -> x0, waiting for transfers between devices: 135 us -> none  [shifted(): lax.ppermute(value, 'rep', [(i, (i + step) % reps) for i in range(reps)])]
    dot_general x6 -> x0, matrix products: 71.2 us -> none  [the longest x3 33.9 us: contract_rows(): lax.dot_general(left, right, (((0,), (0,)), ((), ())), preferred_element_...]
    unnamed x40 -> x20, local copies, waits for them, and re-layouts: 11.8 us -> 0.54 us
    ppermute x8 -> x0, starting transfers between devices: 9.71 us -> none  [shifted(): lax.ppermute(value, 'rep', [(i, (i + step) % reps) for i in range(reps)])]
    dynamic_slice x5 -> x0, local copies, waits for them, and re-layouts: 8.32 us -> none  [columns(): return lax.dynamic_slice_in_dim(value, owner * width, width, axis=1)]
  transfers between devices with their start and end apart: 20 -> 0, of which waited for: 15 -> 0; matrix products, arithmetic and copies ran while one was open for 12% -> 0% of each run, Pallas kernels for 0% -> 0%
where the time goes in v1:
time: 409 us
  Pallas kernels  390 us (95%)
  other arithmetic  18.4 us (4%)
    pallas_call x1, Pallas kernels, fused_device(): pl.pallas_call(functools.partial(fused_kernel, nz), out_shape=(grad, grad...  390 us

profile of v1, /device:TPU:5, one launch (start us, length us, event | category | flops | bytes accessed | tf_op | source)
XLA Modules:
  0.0 409.2 jit_solution(4643914691589304461)
XLA Ops:
  0.6 0.0 copy-start.2
  0.6 0.0 copy-start.4
  0.7 1.7 fusion.8
  2.3 0.7 broadcast_multiply_fusion
  3.0 2.1 fusion.5
  5.1 0.0 copy-start.9
  5.2 0.0 copy-done.2
  5.2 0.0 copy-done.4
  5.2 1.5 fusion.2.branch
  6.7 0.0 copy-done
  6.7 0.0 copy-done.9
  6.7 1.3 fusion.10.normed
  8.0 389.5 %shard_map.129 = (bf16[256,2816]{1,0:T(8,128)(2,1)}, bf16[256,2816]{1,0:T(8,128)(2,1)}, bf16[256,2816]{1,0:T(8,128)(2,1)}, bf16[256,2048]{1,0:T(8,128)(2,1)}, bf16[256,2048]{1,0:T(8,128)(2,1)}) custom-call(bf16[256,2048]{1,0:T(8,128)(2,1)} %fusion.10.normed, bf16[256,2048]{1,0:T(8,128)(2,1)} %fusion.2.branch, bf16[512,2816]{1,0:T(8,128)(2,1)} %gate.1, ...), custom_call_target="tpu_custom_call" | custom-call | tf_op jit(solution)/shard_map/pallas_call | solution.py:768
  397.5 0.0 copy-start.1
  397.5 0.0 copy-start.3
  397.6 0.0 copy-start.5
  397.6 2.6 fusion.12
  400.2 0.2 copy-done.5
  400.3 3.2 fusion.4
  403.5 1.8 convert_element_type.42
  405.3 0.2 copy-done.7
  405.5 1.8 convert_element_type.43
  407.2 0.2 copy-done.6
  407.4 1.8 convert_element_type.44
  (10 shorter events, 0.0 us)
Async XLA Ops:
  0.6 4.5 %copy-start.2 = (bf16[256,2048]{1,0:T(8,128)(2,1)S(1)}, bf16[256,2048]{1,0:T(8,128)(2,1)}, u32[]{:S(2)}) copy-start(bf16[256,2048]{1,0:T(8,128)(2,1)} %param.16) | copy-start | bytes 3145732
  0.6 4.5 %copy-start.4 = (bf16[256,2048]{1,0:T(8,128)(2,1)S(1)}, bf16[256,2048]{1,0:T(8,128)(2,1)}, u32[]{:S(2)}) copy-start(bf16[256,2048]{1,0:T(8,128)(2,1)} %param.15) | copy-start | bytes 3145732
  5.1 1.6 copy-start
  5.1 1.6 copy-start.9
  397.5 2.6 copy-start.1
  397.5 2.6 copy-start.3
  397.6 2.8 copy-start.5
  400.3 3.2 copy-start.8
  403.5 1.9 copy-start.7
  405.5 1.9 copy-start.6

commit v2 on v1

--- a/solution.py
+++ b/solution.py
@@ -9,7 +9,8 @@
 
 eps = 1e-06
 bf16, f32 = jnp.bfloat16, jnp.float32
-SEMS, LOCALS = 200, 64
+SEMS, LOCALS = 240, 64
+CHUNKS = 3
 
 
 def contract_rows(left, right):
@@ -175,8 +176,11 @@
 
 def fused_kernel(
     nz,
-    normed,
+    inputs,
     branch,
+    cotangent,
+    pre_gain,
+    post_gain,
     gate,
     up,
     down_w,
@@ -185,16 +189,15 @@
     down_out,
     gate_out,
     up_out,
-    sum_own,
-    sum_far,
+    rows_out,
     rows,
     acts,
     weights,
     parts,
-    halves,
     near,
     mate,
     side,
+    distant,
     tile,
     send,
     recv,
@@ -210,14 +213,15 @@
     to_up, to_dn = {"fs": f + 2}, {"fs": f - 2}
     has_up, has_dn = z < nz - 1, z > 0
 
-    tokens, model = normed.shape
+    tokens, model = inputs.shape
     chip = gate.shape[0]
     feats = down_w.shape[0]
     block = 2 * feats
     half = gate.shape[1] // 2
     full = acts.shape[2]
     main = full - LANE
-    cut = full // 2
+    cut = full // CHUNKS
+    tail = CHUNKS - 1
     wide, slim = y == c, y != c
     sources = (down_w, gate_w, up_w)
     outs = (down_out, gate_out, up_out)
@@ -273,40 +277,48 @@
     def slot_rows(slot, core):
         return pl.ds((slot * 2 + core) * tokens, tokens)
 
-    own_rows = [
-        links.here(branch, rows.at[0, slot_rows(0, c), :]),
-        links.here(normed, rows.at[1, slot_rows(0, c), :]),
-    ]
+    own_rows = [links.here(v, near.at[i]) for i, v in enumerate((branch, cotangent, inputs))]
+
+    def make_rows(a):
+        @pl.loop(0, tokens // 16)
+        def _(i):
+            at = pl.ds(i * 16, 16)
+            v = near[0 if a == 0 else 2, at, :].astype(f32)
+            inv = lax.rsqrt(jnp.mean(v * v, axis=-1, keepdims=True) + eps)
+            if a == 0:
+                u = 0.5 * near[1, at, :].astype(f32) * post_gain[...]
+                value = inv * u - v * inv**3 * jnp.mean(u * v, axis=-1, keepdims=True)
+            else:
+                value = v * inv * pre_gain[...]
+            rows[a, pl.ds(c * tokens + i * 16, 16), :] = value.astype(bf16)
 
     pl.semaphore_wait(barrier, 4 + has_up.astype(jnp.int32) + has_dn.astype(jnp.int32))
 
-    tables = (branch, normed)
-    part = model // 2
-
-    def row_cols(h):
-        return pl.ds(h * part, part)
+    splits = (model, model // 2)
+
+    def row_cols(a, kind):
+        first = kind in ("y1", "x2", "x3")
+        return pl.ds(0, splits[a]) if first else pl.ds(splits[a], model - splits[a])
+
+    def half_cols(h):
+        return pl.ds(h * (model // 2), model // 2)
 
     def row_send(a, kind):
-        h = 0 if kind in ("y1", "x2", "x3") else 1
         device = to_y if kind[0] == "y" else to_x
-        if kind in ("x3", "y3"):
-            source = rows.at[a, slot_rows(1 if kind == "x3" else 2, c), row_cols(h)]
-            target = 3
-        else:
-            source = tables[a].at[:, row_cols(h)]
-            target = 1 if kind[0] == "y" else 2
-        links.start(f"r{a}{kind}", source, rows.at[a, slot_rows(target, c), row_cols(h)], device)
+        relay = {"x3": 1, "y3": 2}
+        target = 3 if kind in relay else (1 if kind[0] == "y" else 2)
+        source = rows.at[a, slot_rows(relay.get(kind, 0), c), row_cols(a, kind)]
+        there = rows.at[a, slot_rows(target, c), row_cols(a, kind)]
+        links.start(f"r{a}{kind}", source, there, device)
 
     def row_wait(a, kind):
-        h = 0 if kind in ("y1", "x2", "x3") else 1
         device = to_y if kind[0] == "y" else to_x
         target = 3 if kind in ("x3", "y3") else (1 if kind[0] == "y" else 2)
-        links.arrive(f"r{a}{kind}", rows.at[a, slot_rows(target, c), row_cols(h)], device)
+        links.arrive(f"r{a}{kind}", rows.at[a, slot_rows(target, c), row_cols(a, kind)], device)
 
     def mate_send(a, slot):
         where = rows.at[a, slot_rows(slot, c), :]
-        source = tables[a] if slot == 0 else where
-        links.start(f"m{a}{slot}", source, where, to_c)
+        links.start(f"m{a}{slot}", where, where, to_c)
 
     def mate_wait(a, slot):
         links.arrive(f"m{a}{slot}", rows.at[a, slot_rows(slot, 1 - c), :], to_c)
@@ -341,32 +353,42 @@
             when = size & has_dn & (z + hop < nz)
             links.start(f"z{w}{o}d{hop}", behind, behind, to_dn, when)
 
-    def z_wait(w, o, hop):
-        for width, size in ((full, wide), (main, slim)):
+    def z_wait(w, o, hop, here):
+        for width, size in ((full, wide & here), (main, slim & here)):
             ahead = weight_piece(w, jnp.maximum(z - hop, 0), o, width)
             links.arrive(f"z{w}{o}u{hop - 1}", ahead, to_up, size & (z >= hop))
             behind = weight_piece(w, jnp.minimum(z + hop, nz - 1), o, width)
             links.arrive(f"z{w}{o}d{hop - 1}", behind, to_dn, size & (z + hop < nz))
 
+    ends = (z == 0) | (z == nz - 1)
+    inner = jnp.logical_not(ends)
+
     def z_step(w, o, hop):
-        z_wait(w, o, hop)
-        if hop < nz - 1:
-            z_send(w, o, hop)
+        z_wait(w, o, hop, inner)
+        z_send(w, o, hop)
+
+    def z_rest(w):
+        for o in range(2):
+            for hop in range(1, nz - 1):
+                z_wait(w, o, hop, ends)
+            z_wait(w, o, nz - 1, ends | inner)
 
     peers = ((2, to_x, 1 - x, y), (1, to_y, x, 1 - y), (3, to_d, 1 - x, 1 - y))
 
-    def act_send(q):
+    def act_send(q, slots):
         for slot, device, xx, yy in peers:
+            if slot not in slots:
+                continue
             for g, saved in ((1, gate), (2, up)):
                 there = acts.at[g, pl.ds(slot * chip, chip), :]
-                lo, hi = (0, cut) if q == 0 else (cut, main)
+                lo, hi = q * cut, min((q + 1) * cut, main)
                 links.start(
                     f"a{q}{g}{slot}",
                     saved.at[:, own_cols(xx, yy, lo, hi)],
                     there.at[:, pl.ds(lo, hi - lo)],
                     device,
                 )
-                if q == 1:
+                if q == tail:
                     links.start(
                         f"e{g}{slot}",
                         saved.at[:, extra_cols(xx)],
@@ -379,9 +401,9 @@
         for slot, device, _, _ in peers:
             for g in (1, 2):
                 there = acts.at[g, pl.ds(slot * chip, chip), :]
-                lo, hi = (0, cut) if q == 0 else (cut, main)
+                lo, hi = q * cut, min((q + 1) * cut, main)
                 links.arrive(f"a{q}{g}{slot}", there.at[:, pl.ds(lo, hi - lo)], device)
-                if q == 1:
+                if q == tail:
                     links.arrive(f"e{g}{slot}", there.at[:, pl.ds(main, LANE)], device, wide)
 
     total = acts.shape[1]
@@ -435,9 +457,9 @@
                 acts[g, :, cols],
             )
 
-        sizes = ((cut, (q == 0) | wide), (cut - LANE, (q == 1) & slim))
+        sizes = ((cut, (q < tail) | wide), (cut - LANE, (q == tail) & slim))
         spot = (q * 3 + g) * (nz + 1)
-        count = 6 * (nz + 1)
+        count = 3 * CHUNKS * (nz + 1)
 
         def take(slot, when):
             for width, size in sizes:
@@ -491,7 +513,7 @@
             guarded(far & size, copy.start)
 
     def grad_sent():
-        @pl.loop(0, 6)
+        @pl.loop(0, 3 * CHUNKS)
         def _(i):
             q, g = lax.div(i, 3), lax.rem(i, 3)
             spot = i * (nz + 1)
@@ -499,8 +521,8 @@
             @pl.loop(0, nz)
             def _(d):
                 for width, size in (
-                    (cut, (q == 0) | wide),
-                    (cut - LANE, (q == 1) & slim),
+                    (cut, (q < tail) | wide),
+                    (cut - LANE, (q == tail) & slim),
                 ):
                     copy = links.make(
                         "p",
@@ -514,64 +536,36 @@
 
     out_waits = []
 
-    def mine(g, yy, lo, hi):
-        return lanes(yy * (main + LANE) + lo, hi - lo)
-
     def spread(q, g):
-        lo, hi = (0, cut) if q == 0 else (cut, main)
-
-        @pl.loop(0, feats // 64)
-        def _(i):
-            at = pl.ds(i * 64, 64)
-            src = pl.ds(y * feats + i * 64, 64)
-            halves[g, at, mine(g, y, lo, hi)] = parts[g, z, src, pl.ds(lo, hi - lo)]
-
-        if q == 1:
-
-            @pl.when(wide)
-            def _():
-                @pl.loop(0, feats // 64)
-                def _(i):
-                    at = pl.ds(i * 64, 64)
-                    src = pl.ds(y * feats + i * 64, 64)
-                    halves[g, at, pl.ds(main, LANE)] = parts[g, z, src, pl.ds(main, LANE)]
-
-        send_rows = parts.at[g, z, pl.ds((1 - y) * feats, feats), :]
-        links.start(
-            f"h{q}{g}y", send_rows.at[:, pl.ds(lo, hi - lo)], halves.at[g, :, mine(g, y, lo, hi)], to_y
-        )
-        if q == 1:
-            links.start(
-                f"h{g}e",
-                send_rows.at[:, pl.ds(main, LANE)],
-                halves.at[g, :, pl.ds(main, LANE)],
-                to_y,
-                wide,
-            )
-        leave(q, g, "o", mine(g, y, lo, hi), y * (main + LANE) + lo, hi - lo)
-
-    def leave(q, g, tag, cols, start, size):
-        there = outs[g].at[:, lanes(x * half + start, size)]
-        links.start(f"h{q}{g}{tag}", halves.at[g, :, cols], there, to_x)
-        out_waits.append(links.here(halves.at[g, :, cols], there))
-        back = outs[g].at[:, lanes((1 - x) * half + start, size)]
-        out_waits.append(lambda: links.arrive(f"h{q}{g}{tag}", back, to_x))
-
-    def spread_on(q, g):
-        lo, hi = (0, cut) if q == 0 else (cut, main)
-        links.arrive(f"h{q}{g}y", halves.at[g, :, mine(g, 1 - y, lo, hi)], to_y)
-        leave(q, g, "n", mine(g, 1 - y, lo, hi), (1 - y) * (main + LANE) + lo, hi - lo)
-        if q == 1:
-            links.arrive(f"h{g}e", halves.at[g, :, pl.ds(main, LANE)], to_y, slim)
-            leave(q, g, "e", pl.ds(main, LANE), main, LANE)
-
-    def row_grad(core, target, add):
-        @pl.loop(0, 16)
-        def _(i):
-            k, n = lax.div(i, 4), lax.rem(i, 4)
-            slot = lax.rem(k * 2 + 1, 4) - lax.div(k, 2)
-            at = pl.ds((slot * 2 + core) * tokens, tokens)
-            wide_cols = pl.ds(pl.multiple_of(n * (model // 4), 512), model // 4)
+        lo, hi = q * cut, min((q + 1) * cut, main)
+        pieces = [("o", lo, hi - lo, y * (main + LANE) + lo, (1 - y) * (main + LANE) + lo, None)]
+        if q == tail:
+            pieces.append(("e", main, LANE, main, main, wide))
+        keep = parts.at[g, z, pl.ds(y * feats, feats), :]
+        give = parts.at[g, z, pl.ds((1 - y) * feats, feats), :]
+        for tag, start, size, here, other, when in pieces:
+            name = f"h{q}{g}{tag}"
+            there = outs[g].at[:, lanes(x * half + here, size)]
+            out_waits.append(links.here(keep.at[:, pl.ds(start, size)], there, when))
+            far_side = [(to_x, 1 - x, here, when), (to_y, x, other, slim), (to_d, 1 - x, other, slim)]
+            for i, (device, xx, col, back_when) in enumerate(far_side):
+                source = keep if i == 0 else give
+                links.start(f"{name}{i}", source.at[:, pl.ds(start, size)], there, device, when)
+                back = outs[g].at[:, lanes(xx * half + col, size)]
+                back_when = None if when is None else back_when
+                out_waits.append(
+                    functools.partial(links.arrive, f"{name}{i}", back, device, back_when)
+                )
+
+    def turn(i):
+        return jnp.where(i < 2, 3 - 2 * i, 6 - 2 * i)
+
+    def row_grad(core, slot, target, add):
+        at = pl.ds((slot * 2 + core) * tokens, tokens)
+
+        @pl.loop(0, 4)
+        def _(n):
+            wide_cols = lanes(n * (model // 4), model // 4)
             feat_rows = pl.ds(n * (model // 4), model // 4)
             value = contract_cols(acts[1, at, :], weights[1, feat_rows, :])
             value = value + contract_cols(acts[2, at, :], weights[2, feat_rows, :])
@@ -579,29 +573,104 @@
                 value = value + mate[slot, :, wide_cols].astype(f32)
             target[slot, :, wide_cols] = value.astype(bf16)
 
-    def add_into(target, source):
+    def to_mate(slot):
+        return links.make(
+            "s", near.at[slot], mate.at[slot], to_c, size=4, send_at=slot, recv_at=slot
+        )
+
+    def rows_for_mate(lo, hi):
+        @pl.loop(lo, hi)
+        def _(i):
+            slot = turn(i)
+            row_grad(1 - c, slot, near, False)
+            to_mate(slot).start()
+
+    def rows_here(lo, hi):
+        @pl.loop(lo, hi)
+        def _(i):
+            slot = turn(i)
+            to_mate(slot).wait_recv()
+            row_grad(c, slot, mate, True)
+
+    def pass_on(slot, h):
+        device, at = (to_y, slot // 2) if h == 0 else (to_x, slot % 2)
+        links.start(
+            f"t{slot}{h}", mate.at[slot, :, half_cols(h)], side.at[at, :, half_cols(h)], device
+        )
+
+    def gather_in(slot, h, last):
+        there = slot + (1 if h == 0 else 2)
+        device, at = (to_y, there // 2) if h == 0 else (to_x, there % 2)
+        links.arrive(f"t{there}{h}", side.at[at, :, half_cols(h)], device)
+
         @pl.loop(0, tokens // 32)
         def _(i):
-            at = pl.ds(i * 32, 32)
-            target[at, :] = (target[at, :].astype(f32) + source[at, :].astype(f32)).astype(bf16)
-
-    mate_send(0, 0)
-    mate_send(1, 0)
+            r = pl.ds(i * 32, 32)
+            value = mate[slot, r, half_cols(h)].astype(f32) + side[at, r, half_cols(h)].astype(f32)
+            mate[slot, r, half_cols(h)] = value.astype(bf16)
+
+        if not last:
+            device = to_x if h == 0 else to_y
+            there = distant.at[:, half_cols(h)]
+            links.start(f"u{h}", mate.at[slot, :, half_cols(h)], there, device)
+
+    def reload():
+        @pl.loop(0, 4)
+        def _(slot):
+            to_mate(slot).wait_send()
+
+        return [links.here(v, near.at[i]) for i, v in ((1, cotangent), (2, inputs))]
+
+    def finish_rows(waits):
+        for wait in waits:
+            wait()
+        for h in range(2):
+            device = to_x if h == 0 else to_y
+            links.arrive(f"u{h}", distant.at[:, half_cols(h)], device)
+
+        @pl.loop(0, tokens // 16)
+        def _(i):
+            at = pl.ds(i * 16, 16)
+            grad = mate[0, at, :].astype(f32) + distant[at, :].astype(f32)
+            v = near[2, at, :].astype(f32)
+            inv = lax.rsqrt(jnp.mean(v * v, axis=-1, keepdims=True) + eps)
+            w = grad * pre_gain[...]
+            value = near[1, at, :].astype(f32) + inv * w
+            value = value - v * inv**3 * jnp.mean(w * v, axis=-1, keepdims=True)
+            near[0, at, :] = value.astype(bf16)
+
+        out_waits.append(links.here(near.at[0], rows_out))
+
+    last = nz - 1
+
+    def run(q, g, s, count, when=None):
+        @pl.loop(0, count if when is None else jnp.where(when, count, 0))
+        def _(i):
+            k = s + i
+            grad_step(q, g + lax.div(k, last), lax.rem(k, last))
+
+    def close(q, g):
+        grad_step(q, g, last)
+        spread(q, g)
+
     y_weight(0)
-    for kind in ("y1", "x1", "x2", "y2"):
-        row_send(0, kind)
+    act_send(0, (2,))
     for wait in own_weight[0]:
         wait()
     z_send(0, 0, 0)
+    for wait in own_rows:
+        wait()
+    make_rows(0)
+    row_send(0, "y1")
+    row_send(0, "x2")
+    y_weight(1)
+    y_weight(2)
+    act_send(0, (1,))
+    mate_send(0, 0)
+    make_rows(1)
+    mate_send(1, 0)
     y_weight_wait(0)
     z_send(0, 1, 0)
-    row_wait(0, "x1")
-    row_send(0, "y3")
-    row_wait(0, "y1")
-    row_send(0, "x3")
-    act_send(0)
-    for kind in ("y1", "x1", "x2", "y2"):
-        row_send(1, kind)
 
     @pl.when(slim)
     def _():
@@ -619,127 +688,103 @@
 
     z_step(0, 0, 1)
     z_step(0, 1, 1)
-    row_wait(0, "y2")
+    row_wait(0, "y1")
+    row_send(0, "x3")
+    act_send(0, (3,))
+    for kind in ("y1", "x1", "x2", "y2"):
+        row_send(1, kind)
     mate_send(0, 1)
-    row_wait(0, "x2")
-    mate_send(0, 2)
-    z_step(0, 0, 2)
-    z_step(0, 1, 2)
+    for hop in range(2, last):
+        z_step(0, 0, hop)
+        z_step(0, 1, hop)
     for w in (1, 2):
         for wait in own_weight[w]:
             wait()
         z_send(w, 0, 0)
+    row_wait(0, "x2")
+    mate_send(0, 2)
+    for w in (1, 2):
+        y_weight_wait(w)
+        z_send(w, 1, 0)
     row_wait(0, "x3")
-    row_wait(0, "y3")
     mate_send(0, 3)
-    z_step(0, 0, 3)
-    z_step(0, 1, 3)
-    for w in (1, 2):
-        z_step(w, 0, 1)
-    for wait in own_acts + own_rows:
+    for o in range(2):
+        for w in (1, 2):
+            z_step(w, o, 1)
+    for wait in own_acts:
         wait()
     act_wait(0)
     make_hidden(0)
     for slot in range(4):
         mate_wait(0, slot)
+    run(0, 0, 0, 1)
     row_wait(1, "x1")
     row_send(1, "y3")
     row_wait(1, "y1")
     row_send(1, "x3")
-    y_weight(1)
-    y_weight(2)
-    act_send(1)
-
-    @pl.loop(0, 2)
-    def _(i):
-        grad_step(0, 0, i)
-
-    for w in (1, 2):
-        z_step(w, 0, 2)
+    act_send(1, (1, 2, 3))
+    act_send(2, (1, 2, 3))
+    for hop in range(2, last):
+        for w in (1, 2):
+            z_step(w, 0, hop)
+    run(0, 0, 1, 1)
+    z_rest(0)
     make_cots(0)
-
-    @pl.loop(2, 4)
-    def _(i):
-        grad_step(0, 0, i)
-
-    spread(0, 0)
+    run(0, 0, 2, last - 2)
     row_wait(1, "y2")
     mate_send(1, 1)
     row_wait(1, "x2")
     mate_send(1, 2)
+    for hop in range(2, last):
+        for w in (1, 2):
+            z_step(w, 1, hop)
     row_wait(1, "x3")
     row_wait(1, "y3")
     mate_send(1, 3)
-    for w in (1, 2):
-        z_step(w, 0, 3)
     for slot in range(4):
         mate_wait(1, slot)
-
-    @pl.loop(0, 4)
-    def _(i):
-        grad_step(0, 1 + lax.rem(i, 2), lax.div(i, 2))
-
-    spread_on(0, 0)
-    for w in (1, 2):
-        y_weight_wait(w)
-        z_send(w, 1, 0)
+    run(0, 1, 0, last)
+    run(0, 2, 0, 1)
+    run(0, 2, 1, last - 1, ends)
     act_wait(1)
     make_hidden(1)
-
-    @pl.loop(0, 1)
-    def _(i):
-        grad_step(1, 0, i)
-
     make_cots(1)
-
-    @pl.loop(4, 8)
-    def _(i):
-        grad_step(0, 1 + lax.rem(i, 2), lax.div(i, 2))
-
-    spread(0, 1)
-    spread(0, 2)
-    for w in (1, 2):
-        z_step(w, 1, 1)
-
-    @pl.loop(1, 6)
-    def _(i):
-        grad_step(1, lax.rem(i, 3), lax.div(i, 3))
-
-    spread_on(0, 1)
-    spread_on(0, 2)
-    for w in (1, 2):
-        z_step(w, 1, 2)
-    for w in (1, 2):
-        z_step(w, 1, 3)
-    row_grad(1 - c, near, False)
-    for slot in range(4):
-        links.start(f"s{slot}", near.at[slot], mate.at[slot], to_c)
-
-    @pl.loop(6, 9)
-    def _(i):
-        grad_step(1, lax.rem(i, 3), lax.div(i, 3))
-
-    for slot in range(4):
-        links.arrive(f"s{slot}", mate.at[slot], to_c)
-    row_grad(c, mate, True)
-    for i in range(2):
-        links.start(f"t{i}", mate.at[2 * i + 1], side.at[i], to_y)
-
-    @pl.loop(9, 12)
-    def _(i):
-        grad_step(1, lax.rem(i, 3), lax.div(i, 3))
-
+    run(1, 0, 0, 3 * last, ends)
+    run(0, 2, 1, last - 1, inner)
+    act_wait(2)
+    make_hidden(2)
+    make_cots(2)
+    run(2, 0, 0, 3 * last, ends)
+    run(1, 0, 0, last, inner)
     for g in range(3):
-        spread(1, g)
-    links.arrive("t1", side.at[1], to_y)
-    add_into(mate.at[2], side.at[1])
-    links.start("t2", mate.at[2], sum_far, to_x)
-    links.arrive("t0", side.at[0], to_y)
-    add_into(mate.at[0], side.at[0])
-    out_waits.append(links.here(mate.at[0], sum_own))
-    for g in range(3):
-        spread_on(1, g)
-    links.arrive("t2", sum_far, to_x)
+        close(0, g)
+    z_rest(1)
+    z_rest(2)
+    rows_for_mate(0, 4)
+    run(1, 1, 0, last, inner)
+    close(1, 0)
+    rows_here(0, 2)
+    pass_on(3, 0)
+    pass_on(3, 1)
+    pass_on(1, 0)
+    rows_here(2, 4)
+    pass_on(2, 1)
+    run(1, 2, 0, last, inner)
+    again = reload()
+    close(1, 1)
+    run(2, 0, 0, last, inner)
+    gather_in(2, 0, False)
+    gather_in(1, 1, False)
+    close(1, 2)
+    run(2, 1, 0, last, inner)
+    gather_in(0, 0, True)
+    gather_in(0, 1, True)
+    close(2, 0)
+    run(2, 2, 0, 2, inner)
+    finish_rows(again)
+    close(2, 1)
+    run(2, 2, 2, last - 2, inner)
+    close(2, 2)
     for wait in out_waits:
         wait()
     grad_sent()
@@ -748,38 +793,29 @@
 
 def fused_device(nz, block_input, pre_gain, post_gain, gate_saved, up_saved, branch_saved,
                  out_cotangent, gate_weight, up_weight, down_weight):
-    xfull = block_input.astype(f32)
-    inv_x = lax.rsqrt(jnp.mean(xfull * xfull, axis=-1, keepdims=True) + eps)
-    normed = (xfull * inv_x * pre_gain).astype(bf16)
-    branch = branch_saved.astype(f32)
-    inv_b = lax.rsqrt(jnp.mean(branch * branch, axis=-1, keepdims=True) + eps)
-    upstream = 0.5 * out_cotangent.astype(f32) * post_gain
-    branch_grad = (
-        inv_b * upstream - branch * inv_b**3 * jnp.mean(upstream * branch, axis=-1, keepdims=True)
-    ).astype(bf16)
-
     tokens, model = block_input.shape
     chip, width = gate_saved.shape
     feats = down_weight.shape[0]
-    half = width // 2
-    full = (half // LANE + 1) // 2 * LANE
+    full = (width // 2 // LANE + 1) // 2 * LANE
     grad = jax.ShapeDtypeStruct((feats, width), bf16)
     total = jax.ShapeDtypeStruct((tokens, model), bf16)
-    down_grad, gate_grad, up_grad, sum_own, sum_far = pl.pallas_call(
+    down_grad, gate_grad, up_grad, input_grad = pl.pallas_call(
         functools.partial(fused_kernel, nz),
-        out_shape=(grad, grad, grad, total, total),
-        in_specs=[pl.BlockSpec(memory_space=pl.ANY)] * 7,
-        out_specs=[pl.BlockSpec(memory_space=pl.ANY)] * 5,
+        out_shape=(grad, grad, grad, total),
+        in_specs=[pl.BlockSpec(memory_space=pl.ANY)] * 3
+        + [pl.BlockSpec(memory_space=pltpu.VMEM)] * 2
+        + [pl.BlockSpec(memory_space=pl.ANY)] * 5,
+        out_specs=[pl.BlockSpec(memory_space=pl.ANY)] * 4,
         scratch_shapes=[
             pltpu.VMEM((2, 4 * chip, model), bf16),
             pltpu.VMEM((3, 4 * chip, full), bf16),
             pltpu.VMEM((3, model, full), bf16),
             pltpu.VMEM((3, nz + 1, 2 * feats, full), bf16),
-            pltpu.VMEM((3, feats, half), bf16),
             pltpu.VMEM((4, tokens, model), bf16),
             pltpu.VMEM((4, tokens, model), bf16),
             pltpu.VMEM((2, tokens, model), bf16),
-            pltpu.VMEM((2 * feats, full // 2), f32),
+            pltpu.VMEM((tokens, model), bf16),
+            pltpu.VMEM((2 * feats, full // CHUNKS), f32),
             pltpu.SemaphoreType.DMA((SEMS,)),
             pltpu.SemaphoreType.DMA((SEMS,)),
             pltpu.SemaphoreType.DMA((LOCALS,)),
@@ -787,17 +823,21 @@
         compiler_params=pltpu.CompilerParams(
             collective_id=0, has_side_effects=True, vmem_limit_bytes=66_900_000
         ),
-    )(normed, branch_grad, gate_saved, up_saved, down_weight, gate_weight, up_weight)
-
-    normed_grad = sum_own.astype(f32) + sum_far.astype(f32)
-    scaled = normed_grad * pre_gain
-    input_grad = (
-        out_cotangent.astype(f32)
-        + inv_x * scaled
-        - xfull * inv_x**3 * jnp.mean(scaled * xfull, axis=-1, keepdims=True)
+    )(
+        block_input,
+        branch_saved,
+        out_cotangent,
+        pre_gain.reshape(1, model),
+        post_gain.reshape(1, model),
+        gate_saved,
+        up_saved,
+        down_weight,
+        gate_weight,
+        up_weight,
     )
+
     return (
-        input_grad.astype(bf16),
+        input_grad,
         gate_grad.astype(f32),
         up_grad.astype(f32),
         down_grad.astype(f32),
@@ -811,7 +851,7 @@
         width = args[3].shape[1] // shape["tp"]
         tiles, odd = divmod(width // 2, LANE)
         fits = shape["rep"] == 2 and shape["tp"] == 2 and shape["fs"] % 2 == 0
-        fits = fits and width % 2 == 0 and odd == 0 and tiles % 4 == 3
+        fits = fits and width % 2 == 0 and odd == 0 and tiles % 6 == 5
         if fits:
             per_device = functools.partial(fused_device, shape["fs"] // 2)
         else:

time: 409 us -> 266 us (0.65)
  Pallas kernels: 390 us -> 255 us
  other arithmetic: 18.4 us -> 6.77 us
    pallas_call x1, Pallas kernels: 390 us -> 255 us  [fused_device(): pl.pallas_call(functools.partial(fused_kernel, nz), out_shape=(grad, grad...]
    reduce_sum x3 -> x0, other arithmetic: 6.34 us -> none  [the longest x1 2.58 us: fused_device(): jnp.mean(scaled * xfull, axis=-1, keepdims=True)]
    convert_element_type x3 -> x0, other arithmetic: 6.01 us -> none  [the longest x1 3.19 us: fused_device(): input_grad.astype(bf16)]
where the time goes in v2:
time: 266 us; the launch traced here: 263 us
  Pallas kernels  255 us (96%)
  other arithmetic  6.77 us (3%)
    pallas_call x1, Pallas kernels, fused_device(): pl.pallas_call(functools.partial(fused_kernel, nz), out_shape=(grad, grad...  255 us

profile of v2, /device:TPU:5, one launch (start us, length us, event | category | flops | bytes accessed | tf_op | source)
XLA Modules:
  0.0 263.4 jit_solution(3184132526420561213)
XLA Ops:
  0.6 254.8 %shard_map.129 = (bf16[256,2816]{1,0:T(8,128)(2,1)}, bf16[256,2816]{1,0:T(8,128)(2,1)}, bf16[256,2816]{1,0:T(8,128)(2,1)}, bf16[256,2048]{1,0:T(8,128)(2,1)}) custom-call(bf16[256,2048]{1,0:T(8,128)(2,1)} %inputs.1, bf16[256,2048]{1,0:T(8,128)(2,1)} %branch.1, bf16[256,2048]{1,0:T(8,128)(2,1)} %cotangent.1, f32[1,2048]{1,0:T(1,128)} %bitcast.2, ...), custom_call_target="tpu_custom_call" | custom-call | tf_op jit(solution)/shard_map/pallas_call | solution.py:802
  255.4 0.0 copy-start.1
  255.4 3.2 %convert_element_type.9 = f32[256,2816]{1,0:T(8,128)} convert(bf16[256,2816]{1,0:T(8,128)(2,1)} %get-tuple-element.9) | non-fusion elementwise | flops 720896 | bytes 4325376 | tf_op jit(solution)/shard_map/convert_element_type | solution.py:841
  258.7 0.0 copy-done.1
  258.7 0.0 copy-start
  258.7 1.8 convert_element_type.10
  260.4 0.2 copy-done
  260.6 0.0 copy-start.2
  260.6 1.8 convert_element_type.11
  262.4 0.0 copy-done.2
  262.4 1.0 copy.15
Async XLA Ops:
  255.4 3.2 %copy-start.1 = (bf16[256,2816]{1,0:T(8,128)(2,1)S(1)}, bf16[256,2816]{1,0:T(8,128)(2,1)}, u32[]{:S(2)}) copy-start(bf16[256,2816]{1,0:T(8,128)(2,1)} %get-tuple-element.10) | copy-start | bytes 4325380
  258.7 1.9 copy-start
  260.6 1.8 copy-start.2

commit v3 on v2

--- a/solution.py
+++ b/solution.py
@@ -11,6 +11,7 @@
 bf16, f32 = jnp.bfloat16, jnp.float32
 SEMS, LOCALS = 240, 64
 CHUNKS = 3
+LINE = 4
 
 
 def contract_rows(left, right):
@@ -292,36 +293,61 @@
                 value = v * inv * pre_gain[...]
             rows[a, pl.ds(c * tokens + i * 16, 16), :] = value.astype(bf16)
 
+        for k in range(nz):
+            mate_send(a, k, 0)
+
     pl.semaphore_wait(barrier, 4 + has_up.astype(jnp.int32) + has_dn.astype(jnp.int32))
 
-    splits = (model, model // 2)
-
-    def row_cols(a, kind):
-        first = kind in ("y1", "x2", "x3")
-        return pl.ds(0, splits[a]) if first else pl.ds(splits[a], model - splits[a])
+    def order(s):
+        def low(zz):
+            return jnp.where(
+                s < nz - 1 - zz, nz - 1 - s, jnp.where(s == nz - 1, zz, s - (nz - 1 - zz))
+            )
+
+        return jnp.where(2 * z < nz, low(z), nz - 1 - low(nz - 1 - z))
+
+    routes = (("y", "y", "y", "y"), ("x", "y", "x", "y"))
 
     def half_cols(h):
         return pl.ds(h * (model // 2), model // 2)
 
-    def row_send(a, kind):
-        device = to_y if kind[0] == "y" else to_x
-        relay = {"x3": 1, "y3": 2}
-        target = 3 if kind in relay else (1 if kind[0] == "y" else 2)
-        source = rows.at[a, slot_rows(relay.get(kind, 0), c), row_cols(a, kind)]
-        there = rows.at[a, slot_rows(target, c), row_cols(a, kind)]
-        links.start(f"r{a}{kind}", source, there, device)
-
-    def row_wait(a, kind):
-        device = to_y if kind[0] == "y" else to_x
-        target = 3 if kind in ("x3", "y3") else (1 if kind[0] == "y" else 2)
-        links.arrive(f"r{a}{kind}", rows.at[a, slot_rows(target, c), row_cols(a, kind)], device)
-
-    def mate_send(a, slot):
-        where = rows.at[a, slot_rows(slot, c), :]
-        links.start(f"m{a}{slot}", where, where, to_c)
-
-    def mate_wait(a, slot):
-        links.arrive(f"m{a}{slot}", rows.at[a, slot_rows(slot, 1 - c), :], to_c)
+    def row_part(a, k, slot, core):
+        return rows.at[a, slot_rows(slot, core), lanes(order(k) * block, block)]
+
+    def row_path(a, k):
+        y_way, x_way = (to_y, 1), (to_x, 2)
+        return (y_way, x_way) if routes[a][k] == "y" else (x_way, y_way)
+
+    def row_first(a, k):
+        (device, slot), _ = row_path(a, k)
+        links.start(f"f{a}{k}", row_part(a, k, 0, c), row_part(a, k, slot, c), device)
+
+    def row_other(a, k):
+        _, (device, slot) = row_path(a, k)
+        links.start(f"o{a}{k}", row_part(a, k, 0, c), row_part(a, k, slot, c), device)
+
+    def row_relay(a, k):
+        (device, slot), (onward, _) = row_path(a, k)
+        links.arrive(f"f{a}{k}", row_part(a, k, slot, c), device)
+        links.start(f"r{a}{k}", row_part(a, k, slot, c), row_part(a, k, 3, c), onward)
+        mate_send(a, k, slot)
+
+    def row_other_in(a, k):
+        _, (device, slot) = row_path(a, k)
+        links.arrive(f"o{a}{k}", row_part(a, k, slot, c), device)
+        mate_send(a, k, slot)
+
+    def row_last_in(a, k):
+        _, (onward, _) = row_path(a, k)
+        links.arrive(f"r{a}{k}", row_part(a, k, 3, c), onward)
+        mate_send(a, k, 3)
+
+    def mate_send(a, k, slot):
+        links.start(f"m{a}{k}{slot}", row_part(a, k, slot, c), row_part(a, k, slot, c), to_c)
+
+    def row_ready(a, k):
+        for slot in range(4):
+            links.arrive(f"m{a}{k}{slot}", row_part(a, k, slot, 1 - c), to_c)
 
     def y_weight(w):
         there = weights.at[w, my_feats, :]
@@ -375,9 +401,9 @@
 
     peers = ((2, to_x, 1 - x, y), (1, to_y, x, 1 - y), (3, to_d, 1 - x, 1 - y))
 
-    def act_send(q, slots):
+    def act_send(q, to):
         for slot, device, xx, yy in peers:
-            if slot not in slots:
+            if slot != to:
                 continue
             for g, saved in ((1, gate), (2, up)):
                 there = acts.at[g, pl.ds(slot * chip, chip), :]
@@ -438,14 +464,6 @@
                 acts[1, sub, cols] = (grad * u * s * (1.0 + g * (1.0 - s))).astype(bf16)
                 acts[2, sub, cols] = (grad * (g * s)).astype(bf16)
 
-    def order(s):
-        def low(zz):
-            return jnp.where(
-                s < nz - 1 - zz, nz - 1 - s, jnp.where(s == nz - 1, zz, s - (nz - 1 - zz))
-            )
-
-        return jnp.where(2 * z < nz, low(z), nz - 1 - low(nz - 1 - z))
-
     def grad_step(q, g, s):
         d = order(s)
         cols = lanes(q * cut, cut)
@@ -536,26 +554,31 @@
 
     out_waits = []
 
+    def out_pieces(q, yy, extra):
+        lo, hi = q * cut, min((q + 1) * cut, main)
+        pieces = [("o", lo, hi - lo, yy * (main + LANE) + lo, None)]
+        if q == tail:
+            pieces.append(("e", main, LANE, main, extra))
+        return pieces
+
     def spread(q, g):
-        lo, hi = q * cut, min((q + 1) * cut, main)
-        pieces = [("o", lo, hi - lo, y * (main + LANE) + lo, (1 - y) * (main + LANE) + lo, None)]
-        if q == tail:
-            pieces.append(("e", main, LANE, main, main, wide))
         keep = parts.at[g, z, pl.ds(y * feats, feats), :]
         give = parts.at[g, z, pl.ds((1 - y) * feats, feats), :]
-        for tag, start, size, here, other, when in pieces:
-            name = f"h{q}{g}{tag}"
-            there = outs[g].at[:, lanes(x * half + here, size)]
+        for tag, start, size, col, when in out_pieces(q, y, wide):
+            there = outs[g].at[:, lanes(x * half + col, size)]
+            back = outs[g].at[:, lanes((1 - x) * half + col, size)]
             out_waits.append(links.here(keep.at[:, pl.ds(start, size)], there, when))
-            far_side = [(to_x, 1 - x, here, when), (to_y, x, other, slim), (to_d, 1 - x, other, slim)]
-            for i, (device, xx, col, back_when) in enumerate(far_side):
-                source = keep if i == 0 else give
-                links.start(f"{name}{i}", source.at[:, pl.ds(start, size)], there, device, when)
-                back = outs[g].at[:, lanes(xx * half + col, size)]
-                back_when = None if when is None else back_when
-                out_waits.append(
-                    functools.partial(links.arrive, f"{name}{i}", back, device, back_when)
-                )
+            links.start(f"h{q}{g}{tag}x", keep.at[:, pl.ds(start, size)], there, to_x, when)
+            links.start(f"h{q}{g}{tag}y", give.at[:, pl.ds(start, size)], there, to_y, when)
+            out_waits.append(functools.partial(links.arrive, f"h{q}{g}{tag}x", back, to_x, when))
+
+    def spread_on(q, g):
+        for tag, start, size, col, when in out_pieces(q, 1 - y, slim):
+            here = outs[g].at[:, lanes(x * half + col, size)]
+            back = outs[g].at[:, lanes((1 - x) * half + col, size)]
+            links.arrive(f"h{q}{g}{tag}y", here, to_y, when)
+            links.start(f"h{q}{g}{tag}n", here, here, to_x, when)
+            out_waits.append(functools.partial(links.arrive, f"h{q}{g}{tag}n", back, to_x, when))
 
     def turn(i):
         return jnp.where(i < 2, 3 - 2 * i, 6 - 2 * i)
@@ -641,152 +664,208 @@
 
         out_waits.append(links.here(near.at[0], rows_out))
 
-    last = nz - 1
-
-    def run(q, g, s, count, when=None):
-        @pl.loop(0, count if when is None else jnp.where(when, count, 0))
-        def _(i):
-            k = s + i
-            grad_step(q, g + lax.div(k, last), lax.rem(k, last))
-
-    def close(q, g):
-        grad_step(q, g, last)
-        spread(q, g)
-
+    def grads(steps, when=None):
+        @pl.loop(0, len(steps) if when is None else jnp.where(when, len(steps), 0))
+        def _(i):
+            k = steps[0]
+            for j in range(1, len(steps)):
+                k = jnp.where(i == j, steps[j], k)
+            k = k + 0 * i
+            grad_step(lax.div(k, 3 * nz), lax.rem(lax.div(k, nz), 3), lax.rem(k, nz))
+
+    def settle(waits):
+        for wait in waits:
+            wait()
+
+    def z_first(w, o):
+        if o == 0:
+            settle(own_weight[w])
+        else:
+            y_weight_wait(w)
+        z_send(w, o, 0)
+
+    def clear_extra():
+        @pl.when(slim)
+        def _():
+            @pl.loop(0, total // 64)
+            def _(i):
+                at = pl.ds(i * 64, 64)
+                for g in (1, 2):
+                    acts[g, at, pl.ds(main, LANE)] = jnp.zeros((64, LANE), bf16)
+
+            @pl.loop(0, model // 64)
+            def _(i):
+                at = pl.ds(i * 64, 64)
+                for w in range(3):
+                    weights[w, at, pl.ds(main, LANE)] = jnp.zeros((64, LANE), bf16)
+
+    z_first(0, 0)
+    act_send(2, 2)
     y_weight(0)
-    act_send(0, (2,))
-    for wait in own_weight[0]:
-        wait()
-    z_send(0, 0, 0)
-    for wait in own_rows:
-        wait()
+    settle(own_rows)
     make_rows(0)
-    row_send(0, "y1")
-    row_send(0, "x2")
+    row_other(0, 0)
+    y_weight(2)
+    make_rows(1)
+    clear_extra()
+    row_first(0, 1)
     y_weight(1)
-    y_weight(2)
-    act_send(0, (1,))
-    mate_send(0, 0)
-    make_rows(1)
-    mate_send(1, 0)
-    y_weight_wait(0)
-    z_send(0, 1, 0)
-
-    @pl.when(slim)
-    def _():
-        @pl.loop(0, total // 64)
-        def _(i):
-            at = pl.ds(i * 64, 64)
-            for g in (1, 2):
-                acts[g, at, pl.ds(main, LANE)] = jnp.zeros((64, LANE), bf16)
-
-        @pl.loop(0, model // 64)
-        def _(i):
-            at = pl.ds(i * 64, 64)
-            for w in range(3):
-                weights[w, at, pl.ds(main, LANE)] = jnp.zeros((64, LANE), bf16)
-
+    row_first(0, 0)
+    row_other(0, 2)
+    row_first(0, 3)
+    z_first(1, 0)
+    row_first(0, 2)
     z_step(0, 0, 1)
+    act_send(0, 2)
+    z_first(2, 0)
+    row_other(0, 3)
+    row_relay(0, 1)
+    act_send(2, 3)
+    row_other(0, 1)
+    z_first(0, 1)
+    row_other_in(0, 0)
+    act_send(2, 1)
+    act_send(0, 1)
+    z_step(0, 0, 2)
     z_step(0, 1, 1)
-    row_wait(0, "y1")
-    row_send(0, "x3")
-    act_send(0, (3,))
-    for kind in ("y1", "x1", "x2", "y2"):
-        row_send(1, kind)
-    mate_send(0, 1)
-    for hop in range(2, last):
-        z_step(0, 0, hop)
-        z_step(0, 1, hop)
-    for w in (1, 2):
-        for wait in own_weight[w]:
-            wait()
-        z_send(w, 0, 0)
-    row_wait(0, "x2")
-    mate_send(0, 2)
-    for w in (1, 2):
-        y_weight_wait(w)
-        z_send(w, 1, 0)
-    row_wait(0, "x3")
-    mate_send(0, 3)
-    for o in range(2):
-        for w in (1, 2):
-            z_step(w, o, 1)
-    for wait in own_acts:
-        wait()
+    row_last_in(0, 1)
+    row_first(1, 1)
+    act_send(0, 3)
+    z_first(2, 1)
+    row_other(1, 0)
+    z_step(0, 1, 2)
+    row_other_in(0, 3)
+    z_first(1, 1)
+    z_step(2, 0, 1)
+    row_other_in(0, 1)
+    row_relay(0, 0)
+    row_relay(0, 3)
+    row_last_in(0, 0)
+    settle(own_acts)
+    act_wait(2)
+    make_hidden(2)
+    z_step(2, 1, 1)
+    z_rest(0)
+    row_first(1, 0)
+    row_ready(0, 1)
+    row_other_in(0, 2)
+    grads((25,), ends)
+    row_relay(0, 2)
+    row_last_in(0, 3)
+    row_ready(0, 0)
+    grads((24,), ends)
     act_wait(0)
     make_hidden(0)
-    for slot in range(4):
-        mate_wait(0, slot)
-    run(0, 0, 0, 1)
-    row_wait(1, "x1")
-    row_send(1, "y3")
-    row_wait(1, "y1")
-    row_send(1, "x3")
-    act_send(1, (1, 2, 3))
-    act_send(2, (1, 2, 3))
-    for hop in range(2, last):
-        for w in (1, 2):
-            z_step(w, 0, hop)
-    run(0, 0, 1, 1)
-    z_rest(0)
+    row_relay(1, 1)
+    row_other(1, 3)
+    row_relay(1, 0)
+    row_ready(0, 3)
+    grads((1,), ends)
+    grads((24,), inner)
+    act_send(1, 1)
+    z_step(1, 1, 1)
+    z_step(2, 0, 2)
+    grads((0,), ends)
+    row_last_in(0, 2)
+    row_other(1, 1)
+    z_step(1, 0, 1)
+    row_ready(0, 2)
+    grads((2,), ends)
+    row_other(1, 2)
     make_cots(0)
-    run(0, 0, 2, last - 2)
-    row_wait(1, "y2")
-    mate_send(1, 1)
-    row_wait(1, "x2")
-    mate_send(1, 2)
-    for hop in range(2, last):
-        for w in (1, 2):
-            z_step(w, 1, hop)
-    row_wait(1, "x3")
-    row_wait(1, "y3")
-    mate_send(1, 3)
-    for slot in range(4):
-        mate_wait(1, slot)
-    run(0, 1, 0, last)
-    run(0, 2, 0, 1)
-    run(0, 2, 1, last - 1, ends)
+    grads((26,), ends)
+    row_other_in(1, 0)
+    grads((25,), inner)
+    row_last_in(1, 1)
+    row_last_in(1, 0)
+    grads((0, 26), inner)
+    act_send(1, 3)
+    make_cots(2)
+    row_other_in(1, 1)
+    row_ready(1, 0)
+    z_step(2, 1, 2)
+    grads((28,), ends)
+    row_first(1, 3)
+    z_step(1, 1, 2)
+    row_ready(1, 1)
+    row_first(1, 2)
+    z_step(1, 0, 2)
+    grads((32, 4, 9, 29, 8), ends)
+    grads((1, 28), inner)
+    row_other_in(1, 3)
+    act_send(1, 2)
+    row_relay(1, 2)
+    grads((33, 5), ends)
+    grads((2, 9, 4, 32), inner)
+    grads((27,))
+    spread(2, 0)
     act_wait(1)
     make_hidden(1)
     make_cots(1)
-    run(1, 0, 0, 3 * last, ends)
-    run(0, 2, 1, last - 1, inner)
-    act_wait(2)
-    make_hidden(2)
-    make_cots(2)
-    run(2, 0, 0, 3 * last, ends)
-    run(1, 0, 0, last, inner)
-    for g in range(3):
-        close(0, g)
+    grads((12, 16, 17), ends)
+    grads((29,), inner)
+    row_other_in(1, 2)
     z_rest(1)
+    row_relay(1, 3)
+    row_last_in(1, 2)
     z_rest(2)
-    rows_for_mate(0, 4)
-    run(1, 1, 0, last, inner)
-    close(1, 0)
+    rows_for_mate(0, 2)
+    grads((3,))
+    spread(0, 0)
+    spread_on(2, 0)
+    rows_for_mate(2, 4)
+    grads((5,), inner)
+    spread_on(0, 0)
     rows_here(0, 2)
     pass_on(3, 0)
     pass_on(3, 1)
     pass_on(1, 0)
+    row_ready(1, 2)
+    grads((30,), ends)
+    grads((12, 8), inner)
+    row_last_in(1, 3)
+    grads((20, 13, 18), ends)
+    grads((6,), inner)
     rows_here(2, 4)
     pass_on(2, 1)
-    run(1, 2, 0, last, inner)
+    grads((34,), ends)
+    row_ready(1, 3)
+    grads((14, 30, 17, 16, 10), inner)
+    gather_in(2, 0, False)
     again = reload()
-    close(1, 1)
-    run(2, 0, 0, last, inner)
-    gather_in(2, 0, False)
+    grads((14,), ends)
     gather_in(1, 1, False)
-    close(1, 2)
-    run(2, 1, 0, last, inner)
+    grads((33,), inner)
+    grads((31,))
+    spread(2, 1)
+    gather_in(0, 1, True)
+    grads((21, 6, 22), ends)
+    grads((13, 34, 18, 20), inner)
+    grads((35,))
+    spread(2, 2)
+    spread_on(2, 1)
+    grads((10,), ends)
+    spread_on(2, 2)
+    grads((19,))
+    spread(1, 1)
+    grads((22,), inner)
+    grads((15,))
+    spread(1, 0)
+    grads((21,), inner)
+    spread_on(1, 1)
+    grads((7,))
+    spread(0, 1)
     gather_in(0, 0, True)
-    gather_in(0, 1, True)
-    close(2, 0)
-    run(2, 2, 0, 2, inner)
     finish_rows(again)
-    close(2, 1)
-    run(2, 2, 2, last - 2, inner)
-    close(2, 2)
-    for wait in out_waits:
-        wait()
+    spread_on(1, 0)
+    grads((23,))
+    spread(1, 2)
+    spread_on(0, 1)
+    grads((11,))
+    spread(0, 2)
+    spread_on(1, 2)
+    spread_on(0, 2)
+    settle(out_waits)
     grad_sent()
     links.finish()
 
@@ -850,7 +929,7 @@
     def run(*args):
         width = args[3].shape[1] // shape["tp"]
         tiles, odd = divmod(width // 2, LANE)
-        fits = shape["rep"] == 2 and shape["tp"] == 2 and shape["fs"] % 2 == 0
+        fits = shape["rep"] == 2 and shape["tp"] == 2 and shape["fs"] == 2 * LINE
         fits = fits and width % 2 == 0 and odd == 0 and tiles % 6 == 5
         if fits:
             per_device = functools.partial(fused_device, shape["fs"] // 2)

time: 266 us -> 256 us (0.962)
  Pallas kernels: 255 us -> 243 us
    pallas_call x1, Pallas kernels: 255 us -> 243 us  [fused_device(): pl.pallas_call(functools.partial(fused_kernel, nz), out_shape=(grad, grad...]
where the time goes in v3:
time: 256 us; the launch traced here: 251 us
  Pallas kernels  243 us (95%)
  other arithmetic  6.77 us (3%)
    pallas_call x1, Pallas kernels, fused_device(): pl.pallas_call(functools.partial(fused_kernel, nz), out_shape=(grad, grad...  243 us

profile of v3, /device:TPU:5, one launch (start us, length us, event | category | flops | bytes accessed | tf_op | source)
XLA Modules:
  0.0 251.4 jit_solution(6433268700752531052)
XLA Ops:
  0.6 242.8 %shard_map.129 = (bf16[256,2816]{1,0:T(8,128)(2,1)}, bf16[256,2816]{1,0:T(8,128)(2,1)}, bf16[256,2816]{1,0:T(8,128)(2,1)}, bf16[256,2048]{1,0:T(8,128)(2,1)}) custom-call(bf16[256,2048]{1,0:T(8,128)(2,1)} %inputs.1, bf16[256,2048]{1,0:T(8,128)(2,1)} %branch.1, bf16[256,2048]{1,0:T(8,128)(2,1)} %cotangent.1, f32[1,2048]{1,0:T(1,128)} %bitcast.2, ...), custom_call_target="tpu_custom_call" | custom-call | tf_op jit(solution)/shard_map/pallas_call | solution.py:881
  243.5 0.0 copy-start.1
  243.5 3.2 %convert_element_type.9 = f32[256,2816]{1,0:T(8,128)} convert(bf16[256,2816]{1,0:T(8,128)(2,1)} %get-tuple-element.9) | non-fusion elementwise | flops 720896 | bytes 4325376 | tf_op jit(solution)/shard_map/convert_element_type | solution.py:920
  246.7 0.0 copy-done.1
  246.7 0.0 copy-start
  246.7 1.8 convert_element_type.10
  248.5 0.2 copy-done
  248.6 0.0 copy-start.2
  248.7 1.8 convert_element_type.11
  250.4 0.0 copy-done.2
  250.4 1.0 copy.15
Async XLA Ops:
  243.5 3.2 %copy-start.1 = (bf16[256,2816]{1,0:T(8,128)(2,1)S(1)}, bf16[256,2816]{1,0:T(8,128)(2,1)}, u32[]{:S(2)}) copy-start(bf16[256,2816]{1,0:T(8,128)(2,1)} %get-tuple-element.10) | copy-start | bytes 4325380
  246.7 1.9 copy-start
  248.6 1.8 copy-start.2

commit v4 on v3

--- a/solution.py
+++ b/solution.py
@@ -571,12 +571,18 @@
             links.start(f"h{q}{g}{tag}x", keep.at[:, pl.ds(start, size)], there, to_x, when)
             links.start(f"h{q}{g}{tag}y", give.at[:, pl.ds(start, size)], there, to_y, when)
             out_waits.append(functools.partial(links.arrive, f"h{q}{g}{tag}x", back, to_x, when))
+            if (q, g) == (0, 2):
+                links.start(f"h{q}{g}{tag}n", give.at[:, pl.ds(start, size)], there, to_d)
+                far = outs[g].at[:, lanes((1 - x) * half + (1 - y) * (main + LANE) + start, size)]
+                out_waits.append(functools.partial(links.arrive, f"h{q}{g}{tag}n", far, to_d))
 
     def spread_on(q, g):
         for tag, start, size, col, when in out_pieces(q, 1 - y, slim):
             here = outs[g].at[:, lanes(x * half + col, size)]
             back = outs[g].at[:, lanes((1 - x) * half + col, size)]
             links.arrive(f"h{q}{g}{tag}y", here, to_y, when)
+            if (q, g) == (0, 2):
+                continue
             links.start(f"h{q}{g}{tag}n", here, here, to_x, when)
             out_waits.append(functools.partial(links.arrive, f"h{q}{g}{tag}n", back, to_x, when))
 

time: 256 us -> 256 us (level)
  no operation moved by 1% of the time
where the time goes in v4:
time: 256 us; the launch traced here: 251 us
  Pallas kernels  243 us (95%)
  other arithmetic  6.77 us (3%)
    pallas_call x1, Pallas kernels, fused_device(): pl.pallas_call(functools.partial(fused_kernel, nz), out_shape=(grad, grad...  243 us

profile of v4, /device:TPU:5, one launch (start us, length us, event | category | flops | bytes accessed | tf_op | source)
XLA Modules:
  0.0 251.4 jit_solution(5680385103016524738)
XLA Ops:
  0.6 242.8 %shard_map.129 = (bf16[256,2816]{1,0:T(8,128)(2,1)}, bf16[256,2816]{1,0:T(8,128)(2,1)}, bf16[256,2816]{1,0:T(8,128)(2,1)}, bf16[256,2048]{1,0:T(8,128)(2,1)}) custom-call(bf16[256,2048]{1,0:T(8,128)(2,1)} %inputs.1, bf16[256,2048]{1,0:T(8,128)(2,1)} %branch.1, bf16[256,2048]{1,0:T(8,128)(2,1)} %cotangent.1, f32[1,2048]{1,0:T(1,128)} %bitcast.2, ...), custom_call_target="tpu_custom_call" | custom-call | tf_op jit(solution)/shard_map/pallas_call | solution.py:887
  243.5 0.0 copy-start.1
  243.5 3.2 %convert_element_type.9 = f32[256,2816]{1,0:T(8,128)} convert(bf16[256,2816]{1,0:T(8,128)(2,1)} %get-tuple-element.9) | non-fusion elementwise | flops 720896 | bytes 4325376 | tf_op jit(solution)/shard_map/convert_element_type | solution.py:926
  246.7 0.0 copy-done.1
  246.7 0.0 copy-start
  246.7 1.8 convert_element_type.10
  248.5 0.2 copy-done
  248.6 0.0 copy-start.2
  248.7 1.8 convert_element_type.11
  250.4 0.0 copy-done.2
  250.4 1.0 copy.15
Async XLA Ops:
  243.5 3.2 %copy-start.1 = (bf16[256,2816]{1,0:T(8,128)(2,1)S(1)}, bf16[256,2816]{1,0:T(8,128)(2,1)}, u32[]{:S(2)}) copy-start(bf16[256,2816]{1,0:T(8,128)(2,1)} %get-tuple-element.10) | copy-start | bytes 4325380
  246.7 1.9 copy-start
  248.6 1.8 copy-start.2
